TPU v7x, 512 devices: a whole 4x8x8 slice. The times are simulated.
512 devices in a mesh: ep: 32 (over z, x), tp: 16 (over y, core).
Axes of the slice: x: 4, y: 8, z: 8, core: 2. Of those that a mesh axis runs over, the one named last changes fastest.
Arguments:
- mixer_input: bfloat16 [16384, 2048], P('ep', 'tp'), may hold values from -6 to 6
- mixer_gain: float32 [2048], replicated, may hold values from 0.1 to 1.9
- w_query: bfloat16 [2048, 1024], P(None, 'tp'), may hold values from -0.125 to 0.125
- w_key: bfloat16 [2048, 128], replicated, may hold values from -0.125 to 0.125
- w_value: bfloat16 [2048, 128], replicated, may hold values from -0.125 to 0.125
- query_gain: float32 [64], replicated, may hold values from 0.5 to 10
- key_gain: float32 [64], replicated, may hold values from 0.5 to 10
- sink_logit: float32 [16], P('tp'), may hold values from 1 to 5
- w_output: bfloat16 [1024, 2048], P('tp'), may hold values from -0.1875 to 0.1875
- expert_input: bfloat16 [4096, 2048], P('ep'), may hold values from -6 to 6
- expert_gain: float32 [2048], replicated, may hold values from 0.1 to 1.9
- route_ids: int32 [4096, 4], P('ep'), may hold values from 0 to 31, all different within a row; in each aligned block of 128 rows (0 to 127, 128 to 255, ...) at most 32 rows name the same one
- route_weight: float32 [4096, 4], P('ep'), may hold values from 0.2 to 1.2
- expert_gate: bfloat16 [32, 2048, 2048], P('ep', None, 'tp'), may hold values from -0.125 to 0.125
- expert_up: bfloat16 [32, 2048, 2048], P('ep', None, 'tp'), may hold values from -0.125 to 0.125
- expert_down: bfloat16 [32, 2048, 2048], P('ep', None, 'tp'), may hold values from -0.125 to 0.125
- shared_gate: bfloat16 [2048, 1024], P(None, 'tp'), may hold values from -0.125 to 0.125
- shared_up: bfloat16 [2048, 1024], P(None, 'tp'), may hold values from -0.125 to 0.125
- shared_down: bfloat16 [1024, 2048], P(None, 'tp'), may hold values from -0.1875 to 0.1875
Outputs:
- mixer_output: bfloat16 [16384, 2048], P('ep', 'tp')
- expert_output: bfloat16 [4096, 2048], P('ep', 'tp')
Inputs may be any that keep to these rules, and one draw needn't show every extreme that they name: `route_ids`: each row names 4 different experts. In the rows of one index of ep (aligned blocks of 128 rows) no expert is named by more than 32 rows, a bound that some block reaches.
All inputs are finite; a program needn't handle non-finite values.
Results may differ from a plain program's by a relative error of at most 0.018.
The roundings to bfloat16 on the way count: a program that leaves them out, or rounds other values in their place, can miss the bound.
Values may be sent and summed in bfloat16 or wider, within the bound.
A program may use at most 64 MiB of HBM per device.

v0:
```python
import jax
import jax.numpy as jnp
from jax import lax
from jax.sharding import PartitionSpec as P

D = 2048
HEAD = 64
KV_HEADS = 2
WINDOW = 128
TOPK = 4


EPSILON = 1e-06


def from_behind(value, axis, steps):
    count = lax.axis_size(axis)
    first, last = (max(0, -steps), min(count, count - steps))
    return lax.ppermute(value, axis, [(source, source + steps) for source in range(first, last)])


def head_norm(matrix, gain_vector):
    return (
        matrix
        * lax.rsqrt(jnp.mean(matrix * matrix, axis=-1, keepdims=True) + EPSILON)
        * gain_vector
    )


def band_attend(queries, keys_own, values_own, keys_prev, values_prev, sink_logit, first_row):
    row_count = queries.shape[0]
    head_count = queries.shape[1]
    blocks = row_count // WINDOW
    keys_all = jnp.concatenate([keys_prev, keys_own], axis=0)
    values_all = jnp.concatenate([values_prev, values_own], axis=0)
    key_band = jnp.concatenate(
        [
            keys_all[:row_count].reshape(blocks, WINDOW, HEAD),
            keys_own.reshape(blocks, WINDOW, HEAD),
        ],
        axis=1,
    )
    value_band = jnp.concatenate(
        [
            values_all[:row_count].reshape(blocks, WINDOW, HEAD),
            values_own.reshape(blocks, WINDOW, HEAD),
        ],
        axis=1,
    )
    query_blocks = queries.reshape(blocks, WINDOW, head_count, HEAD)
    scores = jnp.einsum(
        "nqhd,nkd->nhqk", query_blocks, key_band, preferred_element_type=jnp.float32
    ) * HEAD ** (-0.5)
    query_idx = jnp.arange(WINDOW, dtype=jnp.int32)[:, None]
    key_idx = jnp.arange(2 * WINDOW, dtype=jnp.int32)[None, :]
    relative = query_idx + WINDOW - key_idx
    block_idx = jnp.arange(blocks, dtype=jnp.int32)[:, None, None]
    key_pos = first_row + block_idx * WINDOW - WINDOW + key_idx[None]
    allowed = ((relative >= 0) & (relative < WINDOW))[None] & (key_pos >= 0)
    allowed = allowed[:, None]
    masked = jnp.where(allowed, scores, -jnp.inf)
    sink_column = sink_logit.reshape(1, head_count, 1, 1)
    peak_score = jnp.maximum(jnp.max(masked, axis=-1, keepdims=True), sink_column)
    exponent = jnp.exp(masked - peak_score)
    denominator = jnp.sum(exponent, axis=-1, keepdims=True) + jnp.exp(sink_column - peak_score)
    probability = (exponent / denominator).astype(jnp.bfloat16)
    mixed_rows = jnp.einsum(
        "nhqk,nkd->nqhd", probability, value_band, preferred_element_type=jnp.float32
    )
    return mixed_rows.reshape(row_count, head_count * HEAD).astype(jnp.bfloat16)


def shards(
    mixer_input,
    mixer_gain,
    w_query,
    w_key,
    w_value,
    query_gain,
    key_gain,
    sink_logit,
    w_output,
    expert_input,
    expert_gain,
    route_ids,
    route_weight,
    expert_gate,
    expert_up,
    expert_down,
    shared_gate,
    shared_up,
    shared_down,
):
    tp_count = lax.axis_size("tp")
    ep_count = lax.axis_size("ep")
    rows_local = mixer_input.shape[0]
    heads_local = w_query.shape[1] // HEAD
    kv_index = lax.axis_index("tp") // (tp_count // KV_HEADS)
    key_cols = lax.dynamic_slice_in_dim(w_key, kv_index * HEAD, HEAD, 1)
    value_cols = lax.dynamic_slice_in_dim(w_value, kv_index * HEAD, HEAD, 1)
    portion_float = lax.all_gather(mixer_input, "tp", axis=1, tiled=True).astype(jnp.float32)
    scaled = (portion_float * mixer_gain).astype(jnp.bfloat16)
    query_raw = jnp.dot(scaled, w_query, preferred_element_type=jnp.float32)
    key_raw = jnp.dot(scaled, key_cols, preferred_element_type=jnp.float32)
    value_raw = jnp.dot(scaled, value_cols, preferred_element_type=jnp.float32)
    squares = jnp.sum(portion_float * portion_float, axis=1)
    inv_rms = lax.rsqrt(squares / D + EPSILON)[:, None]
    queries = head_norm(query_raw.reshape(rows_local, heads_local, HEAD), query_gain).astype(
        jnp.bfloat16
    )
    keys_own = head_norm(key_raw, key_gain).astype(jnp.bfloat16)
    values_own = (value_raw * inv_rms).astype(jnp.bfloat16)
    keys_prev, values_prev = from_behind(
        (keys_own[rows_local - WINDOW :], values_own[rows_local - WINDOW :]), "ep", 1
    )
    first_row = lax.axis_index("ep") * rows_local
    attended = band_attend(
        queries, keys_own, values_own, keys_prev, values_prev, sink_logit, first_row
    )
    out_columns = lax.all_to_all(w_output, "tp", split_axis=1, concat_axis=0, tiled=True)
    mixer_output = jnp.dot(
        lax.all_gather(attended, "tp", axis=1, tiled=True),
        out_columns,
        preferred_element_type=jnp.float32,
    ).astype(jnp.bfloat16)
    tokens_local = expert_input.shape[0]
    expert_float = expert_input.astype(jnp.float32)
    normed = (
        expert_float
        * lax.rsqrt(jnp.mean(expert_float * expert_float, axis=-1, keepdims=True) + EPSILON)
        * expert_gain
    ).astype(jnp.bfloat16)
    capacity = 2 * tokens_local * TOPK // ep_count
    flat_ids = route_ids.reshape(-1)
    onehot = (flat_ids[:, None] == jnp.arange(ep_count, dtype=jnp.int32)[None, :]).astype(jnp.int32)
    earlier = jnp.cumsum(onehot, axis=0) - onehot
    slot_index = jnp.sum(earlier * onehot, axis=-1)
    slot_column = flat_ids * capacity + slot_index
    token_ids = jnp.arange(tokens_local * TOPK, dtype=jnp.int32) // TOPK
    slot_table = (
        jnp.full((ep_count * capacity,), tokens_local, jnp.int32).at[slot_column].set(token_ids)
    )
    col_width = expert_down.shape[2]
    arrived_rows = ep_count * capacity
    own_columns = lax.dynamic_slice_in_dim(normed, lax.axis_index("tp") * col_width, col_width, 1)
    padded = jnp.concatenate([own_columns, jnp.zeros((1, col_width), jnp.bfloat16)], axis=0)
    outgoing = padded[slot_table].reshape(ep_count, capacity, col_width)
    arrived = lax.all_to_all(outgoing, "ep", split_axis=0, concat_axis=0, tiled=True).reshape(
        arrived_rows, col_width
    )
    portion = lax.all_gather(arrived, "tp", axis=1, tiled=True)
    gate_part = expert_gate[0]
    up_part = expert_up[0]
    gate_pre = jnp.dot(portion, gate_part, preferred_element_type=jnp.float32)
    up_pre = jnp.dot(portion, up_part, preferred_element_type=jnp.float32)
    routed_hidden = (jax.nn.silu(gate_pre) * up_pre).astype(jnp.bfloat16)
    shared_hidden = (
        jax.nn.silu(jnp.dot(normed, shared_gate, preferred_element_type=jnp.float32))
        * jnp.dot(normed, shared_up, preferred_element_type=jnp.float32)
    ).astype(jnp.bfloat16)
    routed_part = expert_down[0]
    routed_sum = jnp.dot(
        lax.all_gather(routed_hidden, "tp", axis=1, tiled=True),
        routed_part,
        preferred_element_type=jnp.float32,
    )
    shared_sum = jnp.dot(
        lax.all_gather(shared_hidden, "tp", axis=1, tiled=True),
        shared_down,
        preferred_element_type=jnp.float32,
    )
    expert_rows = routed_sum.astype(jnp.bfloat16).reshape(ep_count, capacity, col_width)
    returned = lax.all_to_all(expert_rows, "ep", split_axis=0, concat_axis=0, tiled=True).reshape(
        arrived_rows, col_width
    )
    picked = returned[slot_column].reshape(tokens_local, TOPK, col_width).astype(jnp.float32)
    expert_output = (shared_sum + jnp.sum(picked * route_weight[:, :, None], axis=1)).astype(
        jnp.bfloat16
    )
    return (mixer_output, expert_output)


def solution(mesh):
    in_specs = (
        P("ep", "tp"),
        P(),
        P(None, "tp"),
        P(),
        P(),
        P(),
        P(),
        P("tp"),
        P("tp", None),
        P("ep", None),
        P(),
        P("ep", None),
        P("ep", None),
        P("ep", None, "tp"),
        P("ep", None, "tp"),
        P("ep", None, "tp"),
        P(None, "tp"),
        P(None, "tp"),
        P(None, "tp"),
    )
    out_specs = (P("ep", "tp"), P("ep", "tp"))
    return jax.shard_map(shards, mesh=mesh, in_specs=in_specs, out_specs=out_specs, check_vma=False)
```

profile of v0, /device:TPU:1, one launch (start us, length us, event | category | flops | bytes accessed | tf_op | source)
XLA Modules:
  0.0 250.1 jit_solution(1595230379398990478)
XLA Ops:
  7.2 0.7 broadcast_multiply_fusion
  8.0 0.8 copy.62
  8.8 0.1 eq.29
  8.9 0.1 eq.25
  9.0 1.2 fusion.20
  10.2 0.1 copy.61
  10.3 0.1 mul.182
  10.5 1.2 reduce-window.6
  11.6 0.2 slice_reduce_fusion
  11.9 0.1 fusion.44
  12.0 2.4 scatter_custom_fusion
  14.5 1.2 fusion.22
  15.8 3.2 %gather_fusion = bf16[1024,128]{1,0:T(8,128)(2,1)S(1)} fusion(bf16[129,128]{1,0:T(8,128)(2,1)S(1)} %concatenate.19, s32[1024]{0:T(1024)S(1)} %fusion.50), kind=kCustom, calls=%fused_computation | custom fusion | bytes 528384 | tf_op jit(solution)/shard_map/gather | solution.py:147
  19.0 25.0 %all_to_all.29 = bf16[32,32,128]{2,1,0:T(8,128)(2,1)} all-to-all(bf16[32,32,128]{2,1,0:T(8,128)(2,1)S(1)} %bitcast.110), channel_id=1, replica_groups=mesh['ep'=32,'tp'=16] {'ep'}, dimensions={0} | all-to-all | bytes 524288 | tf_op jit(solution)/shard_map/all_to_all | solution.py:148
  44.1 0.7 all-gather.5.cloned.1.call-update
  44.9 49.5 %all-gather.9.cloned.1.call-done = bf16[1024,2048]{1,0:T(8,128)(2,1)} async-done(((bf16[1024,128]{1,0:T(8,128)(2,1)}), bf16[1024,2048]{1,0:T(8,128)(2,1)}) %all-gather.9.cloned.1.call-update) | async-done | bytes 4194320 | tf_op jit(solution)/shard_map/all_gather | solution.py:151
  94.4 3.6 %fusion.25 = f32[1024,128]{1,0:T(8,128)S(1)} fusion(bf16[1024,2048]{1,0:T(8,128)(2,1)} %all-gather.9.cloned.1.call-done, bf16[1,2048,128]{2,1,0:T(8,128)(2,1)S(1)} %copy-done), kind=kOutput, calls=%fused_computation.32 | convolution fusion | flops 536870912 | bytes 5242880 | tf_op jit(solution)/shard_map/dot_general | solution.py:154
  98.0 2.0 fusion.9
  100.8 0.1 add_compare_fusion
  101.0 36.5 %all-gather.5.cloned.1.call-done = bf16[512,2048]{1,0:T(8,128)(2,1)} async-done(((bf16[512,128]{1,0:T(8,128)(2,1)}), bf16[512,2048]{1,0:T(8,128)(2,1)}) %all-gather.5.cloned.1.call-update) | async-done | bytes 2097168 | tf_op jit(solution)/shard_map/all_gather | solution.py:101
  137.5 2.2 fusion.1
  139.7 2.5 %fusion.14 = bf16[512,64]{0,1:T(8,128)(2,1)S(1)} fusion(bf16[512,2048]{1,0:T(8,128)(2,1)} %all-gather.5.cloned.1.call-done, f32[2048]{0:T(1024)S(1)} %copy-done.8, bf16[2048,128]{1,0:T(8,128)(2,1)S(1)} %copy-done.12, s32[]{:T(128)S(6)} %select_n.36, f32[512]{0:T(512)S(1)} %add_rsqrt_fusion.2), kind=kOutput, calls=%fused_computation.20 | convolution fusion | flops 137428992 | bytes 2697220 | tf_op jit(solution)/shard_map/dot_general | solution.py:105
  142.3 3.1 %collective-permute-start = (bf16[128,64]{0,1:T(8,128)(2,1)S(1)}, bf16[128,64]{0,1:T(8,128)(2,1)S(1)}, u32[]{:S(2)}, u32[]{:S(2)}) collective-permute-start(bf16[128,64]{0,1:T(8,128)(2,1)S(1)} %slice.28), channel_id=1, source_target_pairs={{0,16},{16,32},{32,48},{48,64},{64,80},{80,96},{96,112},{112,128},... | collective-permute-start | bytes 49160 | tf_op jit(solution)/shard_map/ppermute | solution.py:19
  145.4 1.0 multiply_reduce_fusion.1
  146.5 0.1 multiply_convert_fusion.1
  146.6 0.1 copy_bitcast_fusion.2
  146.7 0.8 multiply_reduce_fusion
  147.5 3.1 %collective-permute-start.1 = (bf16[128,64]{0,1:T(8,128)(2,1)S(1)}, bf16[128,64]{0,1:T(8,128)(2,1)S(1)}, u32[]{:S(2)}, u32[]{:S(2)}) collective-permute-start(bf16[128,64]{0,1:T(8,128)(2,1)S(1)} %slice.29), channel_id=1, source_target_pairs={{0,16},{16,32},{32,48},{48,64},{64,80},{80,96},{96,112},{112,128},... | collective-permute-start | bytes 49160 | tf_op jit(solution)/shard_map/ppermute | solution.py:19
  150.7 0.8 collective-permute-done.1
  151.5 0.3 fusion.60
  151.9 0.1 fusion.29
  152.0 0.2 fusion.17
  152.2 0.1 copy.59
  152.3 0.6 copy.88
  152.9 0.8 copy_bitcast_fusion
  153.7 6.4 %all-to-all-start = ((bf16[64,16,128]{2,0,1:T(8,128)(2,1)}), bf16[64,16,128]{2,0,1:T(8,128)(2,1)S(1)}, u32[]{:S(2)}, u32[]{:S(2)}) async-start(bf16[64,16,128]{2,0,1:T(8,128)(2,1)} %copy_bitcast_fusion), calls=%async_computation | async-start | bytes 524288 | tf_op jit(solution)/shard_map/all_to_all | solution.py:120
  160.1 0.3 fusion.61
  160.4 34.8 %all-gather.11.cloned.1.call-done = bf16[1024,2048]{1,0:T(8,128)(2,1)} async-done(((bf16[1024,128]{1,0:T(8,128)(2,1)}), bf16[1024,2048]{1,0:T(8,128)(2,1)}) %all-gather.11.cloned.1.call-update) | async-done | bytes 4194320 | tf_op jit(solution)/shard_map/all_gather | solution.py:163
  195.3 4.2 %convolution_convert_fusion = bf16[1024,128]{1,0:T(8,128)(2,1)} fusion(bf16[1024,2048]{1,0:T(8,128)(2,1)} %all-gather.11.cloned.1.call-done, bf16[1,2048,128]{2,1,0:T(8,128)(2,1)S(1)} %copy-done.13), kind=kOutput, calls=%fused_computation.16 | convolution fusion | flops 537001984 | bytes 4980736 | tf_op jit(solution)/shard_map/dot_general | solution.py:162
  199.5 10.4 %all-to-all-start.2 = ((bf16[32,32,128]{2,1,0:T(8,128)(2,1)}), bf16[32,32,128]{2,1,0:T(8,128)(2,1)S(1)}, u32[]{:S(2)}, u32[]{:S(2)}) async-start(bf16[32,32,128]{2,1,0:T(8,128)(2,1)} %bitcast.16), calls=%async_computation.2 | async-start | bytes 524288 | tf_op jit(solution)/shard_map/all_to_all | solution.py:173
  209.9 0.3 fusion.19
  210.3 0.1 copy.65
  210.4 17.6 %all_gather.17 = bf16[128,1024]{0,1:T(8,128)(2,1)S(1)} all-gather(bf16[128,64]{0,1:T(8,128)(2,1)S(1)} %fusion.19), channel_id=1, replica_groups=mesh['ep'=32,'tp'=16] {'tp'}, dimensions={1}, use_global_device_ids=true | all-gather | bytes 278528 | tf_op jit(solution)/shard_map/all_gather | solution.py:168
  227.9 10.8 %all-gather.7.cloned.1.call-done = bf16[512,1024]{0,1:T(8,128)(2,1)} async-done(((bf16[512,64]{0,1:T(8,128)(2,1)}), bf16[512,1024]{0,1:T(8,128)(2,1)}) %all-gather.7.cloned.1.call-update) | async-done | bytes 1048592 | tf_op jit(solution)/shard_map/all_gather | solution.py:122
  238.7 2.4 convolution_convert_fusion.1
  241.1 1.3 gather_fusion.1
  242.4 0.2 fusion.30
  242.7 0.9 fusion.18
  (65 shorter events, 0.5 us)
Async XLA Ops:
  7.2 87.2 %copy-start = (bf16[1,2048,128]{2,1,0:T(8,128)(2,1)S(1)}, bf16[1,2048,128]{2,1,0:T(8,128)(2,1)}, u32[]{:S(2)}) copy-start(bf16[1,2048,128]{2,1,0:T(8,128)(2,1)} %param.32) | copy-start | bytes 1572868
  7.2 87.2 %all-gather.9.cloned.1.call-start = ((), (), s32[]{:S(2)}) async-start(), calls=%async_computation.5 | async-start | bytes 4456448 | tf_op jit(solution)/shard_map/all_gather | solution.py:151
  19.0 79.0 %copy-start.11 = (bf16[1,2048,128]{2,1,0:T(8,128)(2,1)S(1)}, bf16[1,2048,128]{2,1,0:T(8,128)(2,1)}, u32[]{:S(2)}) copy-start(bf16[1,2048,128]{2,1,0:T(8,128)(2,1)} %param.33) | copy-start | bytes 1572868
  44.1 93.4 %all-gather.5.cloned.1.call-start = ((), (), s32[]{:S(2)}) async-start(), calls=%async_computation.3 | async-start | bytes 2228224 | tf_op jit(solution)/shard_map/all_gather | solution.py:101
  44.8 150.5 %all-gather.11.cloned.1.call-start = ((), (), s32[]{:S(2)}) async-start(), calls=%async_computation.6 | async-start | bytes 4456448 | tf_op jit(solution)/shard_map/all_gather | solution.py:163
  94.4 3.6 %copy-start.2 = (bf16[1024,2048]{1,0:T(8,128)(2,1)S(1)}, bf16[1024,2048]{1,0:T(8,128)(2,1)}, u32[]{:S(2)}) copy-start(bf16[1024,2048]{1,0:T(8,128)(2,1)} %all-gather.9.cloned.1.call-done) | copy-start | bytes 12582916
  98.0 41.7 %copy-start.8 = (f32[2048]{0:T(1024)S(1)}, f32[2048]{0:T(1024)}, u32[]{:S(2)}) copy-start(f32[2048]{0:T(1024)} %param.20) | copy-start | bytes 24580
  98.0 41.7 %copy-start.12 = (bf16[2048,128]{1,0:T(8,128)(2,1)S(1)}, bf16[2048,128]{1,0:T(8,128)(2,1)}, u32[]{:S(2)}) copy-start(bf16[2048,128]{1,0:T(8,128)(2,1)} %param.23) | copy-start | bytes 1572868
  100.0 45.4 %copy-start.3 = (bf16[2048,128]{1,0:T(8,128)(2,1)S(1)}, bf16[2048,128]{1,0:T(8,128)(2,1)}, u32[]{:S(2)}) copy-start(bf16[2048,128]{1,0:T(8,128)(2,1)} %param.22) | copy-start | bytes 1572868
  100.0 46.5 %copy-start.9 = (f32[64]{0:T(128)S(1)}, f32[64]{0:T(128)}, u32[]{:S(2)}) copy-start(f32[64]{0:T(128)} %param.25) | copy-start | bytes 772
  100.0 46.6 %copy-start.14 = (bf16[2048,64]{0,1:T(8,128)(2,1)S(1)}, bf16[2048,64]{0,1:T(8,128)(2,1)}, u32[]{:S(2)}) copy-start(bf16[2048,64]{0,1:T(8,128)(2,1)} %param.21) | copy-start | bytes 786436
  100.0 138.7 %all-gather.7.cloned.1.call-start = ((), (), s32[]{:S(2)}) async-start(), calls=%async_computation.4 | async-start | bytes 1114112 | tf_op jit(solution)/shard_map/all_gather | solution.py:122
  137.5 7.9 %copy-start.1 = (bf16[512,2048]{1,0:T(8,128)(2,1)S(1)}, bf16[512,2048]{1,0:T(8,128)(2,1)}, u32[]{:S(2)}) copy-start(bf16[512,2048]{1,0:T(8,128)(2,1)} %all-gather.5.cloned.1.call-done) | copy-start | bytes 6291460
  139.7 11.8 %copy-start.15 = (f32[64]{0:T(128)S(1)}, f32[64]{0:T(128)}, u32[]{:S(2)}) copy-start(f32[64]{0:T(128)} %param.24) | copy-start | bytes 772
  142.3 8.3 %collective-permute-start = (bf16[128,64]{0,1:T(8,128)(2,1)S(1)}, bf16[128,64]{0,1:T(8,128)(2,1)S(1)}, u32[]{:S(2)}, u32[]{:S(2)}) collective-permute-start(bf16[128,64]{0,1:T(8,128)(2,1)S(1)} %slice.28), channel_id=1, source_target_pairs={{0,16},{16,32},{32,48},{48,64},{64,80},{80,96},{96,112},{112,128},... | collective-permute-start | bytes 49160 | tf_op jit(solution)/shard_map/ppermute | solution.py:19
  146.4 6.5 %copy-start.6 = (bf16[64,2048]{1,0:T(8,128)(2,1)S(1)}, bf16[64,2048]{1,0:T(8,128)(2,1)}, u32[]{:S(2)}) copy-start(bf16[64,2048]{1,0:T(8,128)(2,1)} %param.27) | copy-start | bytes 786436
  146.7 13.5 %copy-start.4 = (bf16[2048,64]{0,1:T(8,128)(2,1)S(1)}, bf16[2048,64]{0,1:T(8,128)(2,1)}, u32[]{:S(2)}) copy-start(bf16[2048,64]{0,1:T(8,128)(2,1)} %param.35) | copy-start | bytes 786436
  146.7 48.6 %copy-start.13 = (bf16[1,2048,128]{2,1,0:T(8,128)(2,1)S(1)}, bf16[1,2048,128]{2,1,0:T(8,128)(2,1)}, u32[]{:S(2)}) copy-start(bf16[1,2048,128]{2,1,0:T(8,128)(2,1)} %param.34) | copy-start | bytes 1572868
  147.5 4.0 %collective-permute-start.1 = (bf16[128,64]{0,1:T(8,128)(2,1)S(1)}, bf16[128,64]{0,1:T(8,128)(2,1)S(1)}, u32[]{:S(2)}, u32[]{:S(2)}) collective-permute-start(bf16[128,64]{0,1:T(8,128)(2,1)S(1)} %slice.29), channel_id=1, source_target_pairs={{0,16},{16,32},{32,48},{48,64},{64,80},{80,96},{96,112},{112,128},... | collective-permute-start | bytes 49160 | tf_op jit(solution)/shard_map/ppermute | solution.py:19
  153.7 56.2 %copy-start.5 = (bf16[2048,64]{0,1:T(8,128)(2,1)S(1)}, bf16[2048,64]{0,1:T(8,128)(2,1)}, u32[]{:S(2)}) copy-start(bf16[2048,64]{0,1:T(8,128)(2,1)} %param.36) | copy-start | bytes 786436
  153.7 45.8 %all-to-all-start = ((bf16[64,16,128]{2,0,1:T(8,128)(2,1)}), bf16[64,16,128]{2,0,1:T(8,128)(2,1)S(1)}, u32[]{:S(2)}, u32[]{:S(2)}) async-start(bf16[64,16,128]{2,0,1:T(8,128)(2,1)} %copy_bitcast_fusion), calls=%async_computation | async-start | bytes 524288 | tf_op jit(solution)/shard_map/all_to_all | solution.py:120
  160.1 50.1 %copy-start.10 = (f32[128,4]{0,1:T(4,128)S(1)}, f32[128,4]{0,1:T(4,128)}, u32[]{:S(2)}) copy-start(f32[128,4]{0,1:T(4,128)} %param.31) | copy-start | bytes 6148
  160.4 82.2 %copy-start.7 = (bf16[1024,128]{1,0:T(8,128)(2,1)S(1)}, bf16[1024,128]{1,0:T(8,128)(2,1)}, u32[]{:S(2)}) copy-start(bf16[1024,128]{1,0:T(8,128)(2,1)} %param.37) | copy-start | bytes 786436
  199.5 41.6 %all-to-all-start.2 = ((bf16[32,32,128]{2,1,0:T(8,128)(2,1)}), bf16[32,32,128]{2,1,0:T(8,128)(2,1)S(1)}, u32[]{:S(2)}, u32[]{:S(2)}) async-start(bf16[32,32,128]{2,1,0:T(8,128)(2,1)} %bitcast.16), calls=%async_computation.2 | async-start | bytes 524288 | tf_op jit(solution)/shard_map/all_to_all | solution.py:173
Sparse Core Ops, SparseCore 0:
  44.2 50.1 all-gather.8
  96.4 41.0 all-gather.4
  139.5 55.7 all-gather.10
  197.8 40.8 all-gather.6
where the time goes:
time: 251 us; the launch traced here: 250 us
  waiting for transfers between devices  133 us (53%)
  blocking collectives  42.6 us (17%)
  starting transfers between devices  23.2 us (9%)
  matrix products  18.5 us (7%)
  between operations  14.9 us (6%)
  local copies, waits for them, and re-layouts  10.2 us (4%)
  other arithmetic  7.45 us (3%)
    all_gather x1, waiting for transfers between devices, shards(): portion = lax.all_gather(arrived, 'tp', axis=1, tiled=True)  49.5 us
    all_gather x1, waiting for transfers between devices, shards(): lax.all_gather(mixer_input, 'tp', axis=1, tiled=True).astype(jnp.float32)  36.5 us
    all_gather x1, waiting for transfers between devices, shards(): lax.all_gather(routed_hidden, 'tp', axis=1, tiled=True)  34.8 us
    all_to_all x1, blocking collectives, shards(): lax.all_to_all(outgoing, 'ep', split_axis=0, concat_axis=0, tiled=True)  25 us
    all_gather x1, blocking collectives, shards(): lax.all_gather(shared_hidden, 'tp', axis=1, tiled=True)  17.6 us
    all_gather x1, waiting for transfers between devices, shards(): lax.all_gather(attended, 'tp', axis=1, tiled=True)  10.8 us
    all_to_all x1, starting transfers between devices, shards(): lax.all_to_all(expert_rows, 'ep', split_axis=0, concat_axis=0, tiled=True)  10.4 us
    all_to_all x1, starting transfers between devices, shards(): lax.all_to_all(w_output, 'tp', split_axis=1, concat_axis=0, tiled=True)  6.4 us
  transfers between devices with their start and end apart: 8, of which 5 were waited for; matrix products, arithmetic and copies ran while one was open for 9% of the time, Pallas kernels for 0%

commit v1 on v0

v1 whole, which is shorter than its diff:
```python
import functools

import jax
import jax.numpy as jnp
from jax import lax
from jax.experimental import pallas as pl
from jax.experimental.pallas import tpu as pltpu
from jax.sharding import PartitionSpec as P

HEAD = 64
WINDOW = 128
EPSILON = 1e-06
CORES = 2
X_SIZE = 4
F32 = jnp.float32
BF16 = jnp.bfloat16
MESH = pl.DeviceIdType.MESH


def mod(value, count):
    return lax.rem(value + count, count)


def dot(a, b):
    return jnp.dot(a, b, preferred_element_type=F32)


class Ring:
    def __init__(self, buf, send_sem, recv_sem, y, ny, place, pending):
        self.buf, self.send_sem, self.recv_sem = buf, send_sem, recv_sem
        self.y, self.ny, self.place, self.pending = y, ny, place, pending
        self.subs = send_sem.shape[2]
        self.half = ny // 2
        self.rows = buf.shape[1] // self.subs

    def carries(self, way, distance, sub):
        if distance < self.half:
            return True
        if distance > self.half:
            return False
        return (sub < self.subs // 2) == (way == 0)

    def copy(self, way, distance, sub):
        sign = 1 if way == 0 else -1
        part = mod(self.y - sign * (distance - 1), self.ny)
        rows = pl.ds(sub * self.rows, self.rows)
        return pltpu.make_async_remote_copy(
            src_ref=self.buf.at[part, rows],
            dst_ref=self.buf.at[part, rows],
            send_sem=self.send_sem.at[way, distance - 1, sub],
            recv_sem=self.recv_sem.at[way, distance - 1, sub],
            device_id=self.place(mod(self.y + sign, self.ny)),
            device_id_type=MESH,
        )

    def arrival(self, way, distance, sub):
        sign = 1 if way == 0 else -1
        part = mod(self.y - sign * distance, self.ny)
        rows = pl.ds(sub * self.rows, self.rows)
        return pltpu.make_async_remote_copy(
            src_ref=self.buf.at[part, rows],
            dst_ref=self.buf.at[part, rows],
            send_sem=self.send_sem.at[way, distance - 1, sub],
            recv_sem=self.recv_sem.at[way, distance - 1, sub],
            device_id=self.place(mod(self.y + sign, self.ny)),
            device_id_type=MESH,
        )

    def send(self, distance, sub, way):
        if self.carries(way, distance, sub):
            copy = self.copy(way, distance, sub)
            copy.start()
            self.pending.append(copy)

    def start(self, sub):
        for way in range(2):
            self.send(1, sub, way)

    def serve_one(self, distance, sub, way):
        if self.carries(way, distance, sub):
            self.arrival(way, distance, sub).wait_recv()
            self.send(distance + 1, sub, way)

    def serve(self, distance):
        for sub in range(self.subs):
            for way in range(2):
                self.serve_one(distance, sub, way)

    def arrived(self, distance):
        if distance < self.half:
            return [mod(self.y - distance, self.ny), mod(self.y + distance, self.ny)]
        return [mod(self.y - distance, self.ny)]


def kernel(
    n_ep,
    ny,
    nx,
    x_ref,
    gain_ref,
    wq_ref,
    wk_ref,
    wv_ref,
    qg_ref,
    kg_ref,
    sink_ref,
    wo_ref,
    ei_ref,
    eg_ref,
    ids_ref,
    rw_ref,
    gate_ref,
    up_ref,
    down_ref,
    sg_ref,
    su_ref,
    sd_ref,
    mo_ref,
    eo_ref,
    xg,
    rg,
    hg,
    ag,
    gw,
    uw,
    dw,
    wqs,
    sgs,
    sus,
    wog,
    og,
    er,
    ret,
    normed,
    gacc,
    uacc,
    oacc,
    q0acc,
    q1acc,
    kacc,
    vacc,
    ssq,
    kv,
    sk,
    mos,
    shp,
    xs_sem,
    xr_sem,
    rs_sem,
    rr_sem,
    hs_sem,
    hr_sem,
    as_sem,
    ar_sem,
    local_sem,
    pair_send,
    pair_recv,
    disp_send,
    disp_recv,
    back_send,
    back_recv,
    back_local,
    wo_send,
    wo_recv,
    halo_send,
    halo_recv,
):
    ep = lax.axis_index("ep")
    tp = lax.axis_index("tp")
    y = tp // CORES
    c = lax.rem(tp, CORES)
    other = 1 - c
    half_ny = ny // 2
    rows = x_ref.shape[0] // CORES
    toks = ei_ref.shape[0]
    dim = ei_ref.shape[1]
    cols = dim // ny
    mine = dim // (ny * CORES)
    cap = er.shape[0] // n_ep
    slots = er.shape[0]
    xi = lax.rem(ep, nx)
    pending = []

    def here(place):
        return (ep, place * CORES + c)

    partner = (ep, y * CORES + other)

    barrier = pltpu.get_barrier_semaphore()

    def greet(k, carry):
        target = lax.rem(ep + k, n_ep)
        for core in range(CORES):
            pl.semaphore_signal(
                barrier, inc=1, device_id=(target, y * CORES + core), device_id_type=MESH
            )
        return carry

    lax.fori_loop(1, n_ep, greet, 0)
    for k in range(1, ny):
        pl.semaphore_signal(barrier, inc=1, device_id=here(mod(y + k, ny)), device_id_type=MESH)
    pl.semaphore_signal(barrier, inc=1, device_id=partner, device_id_type=MESH)

    own_lanes = pl.ds(pl.multiple_of(c * mine, mine), mine)
    own_rows = pl.ds(pl.multiple_of(c * rows, rows), rows)
    other_rows = pl.ds(pl.multiple_of(other * rows, rows), rows)
    chip_lanes = pl.ds(pl.multiple_of(y * cols, cols), cols)
    wo_rows = wo_ref.shape[0]
    wo_piece = wo_rows // nx
    wo_src = pl.ds(pl.multiple_of(xi * wo_piece, wo_piece), wo_piece)
    wo_dst = pl.ds(pl.multiple_of(c * wo_rows + xi * wo_piece, wo_piece), wo_piece)
    local = [
        pltpu.make_async_copy(x_ref.at[own_rows], xg.at[y, :, own_lanes], local_sem.at[0]),
        pltpu.make_async_copy(wq_ref, wqs.at[c], local_sem.at[1]),
        pltpu.make_async_copy(sg_ref, sgs.at[c], local_sem.at[2]),
        pltpu.make_async_copy(su_ref, sus.at[c], local_sem.at[3]),
        pltpu.make_async_copy(gate_ref.at[0], gw.at[:, own_lanes], local_sem.at[4]),
        pltpu.make_async_copy(up_ref.at[0], uw.at[:, own_lanes], local_sem.at[5]),
        pltpu.make_async_copy(down_ref.at[0], dw.at[:, own_lanes], local_sem.at[6]),
        pltpu.make_async_copy(
            wo_ref.at[wo_src, chip_lanes],
            wog.at[y, wo_dst],
            local_sem.at[7],
        ),
    ]
    for copy in local:
        copy.start()
    sk[c] = jnp.full((8, 128), sink_ref[0], F32)

    expert_float = ei_ref[...].astype(F32)
    squares = jnp.mean(expert_float * expert_float, axis=-1, keepdims=True)
    normed[...] = (expert_float * lax.rsqrt(squares + EPSILON) * eg_ref[...]).astype(BF16)
    topk = ids_ref.shape[1]
    expert_idx = lax.broadcasted_iota(jnp.int32, (toks, n_ep), 1)
    named = jnp.zeros((toks, n_ep), F32)
    for k in range(topk):
        named = named + jnp.where(ids_ref[:, k : k + 1] == expert_idx, 1.0, 0.0)
    t_row = lax.broadcasted_iota(jnp.int32, (toks, toks), 0)
    t_col = lax.broadcasted_iota(jnp.int32, (toks, toks), 1)
    before = jnp.where(t_col < t_row, 1.0, 0.0).astype(BF16)
    rank = dot(before, named.astype(BF16))
    rank = jnp.where(named > 0.0, rank, -1.0)
    e_row = lax.broadcasted_iota(jnp.int32, (n_ep, slots), 0)
    e_col = lax.broadcasted_iota(jnp.int32, (n_ep, slots), 1)
    spread = jnp.where(e_col // cap == e_row, 1.0, 0.0).astype(BF16)
    slot_lane = lax.rem(lax.broadcasted_iota(jnp.int32, (toks, slots), 1), cap)

    def chosen(half):
        rank_wide = dot(rank.astype(BF16), spread).astype(jnp.int32)
        return rank_wide == slot_lane + half * cap

    pick = jnp.where(chosen(c), 1.0, 0.0).astype(BF16)
    og[...] = lax.dot_general(
        pick, normed[:, chip_lanes], (((0,), (0,)), ((), ())), preferred_element_type=F32
    ).astype(BF16)

    pl.semaphore_wait(barrier, (n_ep - 1) * CORES + (ny - 1) + 1)

    def to_partner(index, source, target):
        copy = pltpu.make_async_remote_copy(
            src_ref=source,
            dst_ref=target,
            send_sem=pair_send.at[index],
            recv_sem=pair_recv.at[index],
            device_id=partner,
            device_id_type=MESH,
        )
        return copy

    def send_partner(index, source, target):
        copy = to_partner(index, source, target)
        copy.start()
        pending.append(copy)

    other_lanes = pl.ds(pl.multiple_of(other * mine, mine), mine)
    send_partner(0, x_ref.at[other_rows], xg.at[y, :, own_lanes])
    x_in = to_partner(0, x_ref.at[other_rows], xg.at[y, :, other_lanes])

    rg_own = pltpu.make_async_copy(
        og.at[pl.ds(pl.multiple_of(ep * cap, cap), cap)],
        rg.at[y, pl.ds(0, cap)],
        disp_recv.at[0],
    )
    rg_own.start()
    r_subs = rs_sem.shape[2]
    per_sub = n_ep // r_subs

    def dispatch(k, carry):
        target = lax.rem(ep + n_ep - k, n_ep)
        pltpu.make_async_remote_copy(
            src_ref=og.at[pl.ds(pl.multiple_of(target * cap, cap), cap)],
            dst_ref=rg.at[y, pl.ds(pl.multiple_of(k * cap, cap), cap)],
            send_sem=disp_send,
            recv_sem=disp_recv.at[k // per_sub],
            device_id=(target, tp),
            device_id_type=MESH,
        ).start()
        return carry

    lax.fori_loop(1, n_ep, dispatch, 0)

    x_ring = Ring(xg, xs_sem, xr_sem, y, ny, here, pending)
    local[0].wait()
    x_in.wait_recv()
    for sub in range(x_ring.subs):
        x_ring.start(sub)

    for k in range(1, ny):
        place = mod(y + k, ny)
        copy = pltpu.make_async_remote_copy(
            src_ref=wo_ref.at[wo_src, pl.ds(pl.multiple_of(place * cols, cols), cols)],
            dst_ref=wog.at[y, wo_dst],
            send_sem=wo_send.at[k - 1],
            recv_sem=wo_recv.at[k - 1],
            device_id=here(place),
            device_id_type=MESH,
        )
        copy.start()
        pending.append(copy)

    send_partner(1, gate_ref.at[0], gw.at[:, own_lanes])
    send_partner(2, up_ref.at[0], uw.at[:, own_lanes])
    send_partner(3, wq_ref, wqs.at[c])
    send_partner(4, sg_ref, sgs.at[c])
    send_partner(5, su_ref, sus.at[c])
    send_partner(6, sk.at[c], sk.at[c])
    send_partner(7, down_ref.at[0], dw.at[:, own_lanes])
    gw_in = to_partner(1, gate_ref.at[0], gw.at[:, other_lanes])
    uw_in = to_partner(2, up_ref.at[0], uw.at[:, other_lanes])
    wq_in = to_partner(3, wq_ref, wqs.at[other])
    sg_in = to_partner(4, sg_ref, sgs.at[other])
    su_in = to_partner(5, su_ref, sus.at[other])
    sk_in = to_partner(6, sk.at[c], sk.at[other])
    dw_in = to_partner(7, down_ref.at[0], dw.at[:, other_lanes])

    for distance in range(1, half_ny + 1):
        x_ring.serve(distance)

    r_ring = Ring(rg, rs_sem, rr_sem, y, ny, here, pending)
    for sub in range(r_subs):
        landed = rg.at[y, pl.ds(sub * per_sub * cap, per_sub * cap)]
        pltpu.make_async_copy(landed, landed, disp_recv.at[sub]).wait()
        r_ring.start(sub)

    for k in range(1, ny):
        place = mod(y + k, ny)
        pltpu.make_async_remote_copy(
            src_ref=wo_ref.at[wo_src, pl.ds(pl.multiple_of(place * cols, cols), cols)],
            dst_ref=wog.at[mod(y - k, ny), wo_dst],
            send_sem=wo_send.at[k - 1],
            recv_sem=wo_recv.at[k - 1],
            device_id=here(place),
            device_id_type=MESH,
        ).wait_recv()
    local[7].wait()

    def wo_leg(k, start):
        place = ep - xi + lax.rem(xi + k, nx)
        source = wo_dst
        if not start:
            sender = lax.rem(xi + nx - k, nx)
            source = pl.ds(pl.multiple_of(c * wo_rows + sender * wo_piece, wo_piece), wo_piece)
        return pltpu.make_async_remote_copy(
            src_ref=wog.at[:, source],
            dst_ref=wog.at[:, source],
            send_sem=wo_send.at[ny - 1 + k - 1],
            recv_sem=wo_recv.at[ny - 1 + k - 1],
            device_id=(place, tp),
            device_id_type=MESH,
        )

    for k in range(1, nx):
        copy = wo_leg(k, True)
        copy.start()
        pending.append(copy)

    for copy in local[1:7]:
        copy.wait()
    wq_in.wait_recv()
    q0acc[...] = jnp.zeros_like(q0acc)
    q1acc[...] = jnp.zeros_like(q1acc)
    kacc[...] = jnp.zeros_like(kacc)
    vacc[...] = jnp.zeros_like(vacc)
    ssq[...] = jnp.zeros_like(ssq)

    def project(part, carry):
        lanes = pl.ds(pl.multiple_of(part * cols, cols), cols)
        portion = xg[part].astype(F32)
        scaled = (portion * gain_ref[:, lanes]).astype(BF16)
        ssq[...] += jnp.sum(portion * portion, axis=-1, keepdims=True)
        q0acc[...] += dot(scaled, wqs[0, lanes, :])
        q1acc[...] += dot(scaled, wqs[1, lanes, :])
        kacc[...] += dot(scaled, wk_ref[lanes, :])
        vacc[...] += dot(scaled, wv_ref[lanes, :])
        return carry

    lax.fori_loop(0, ny, project, 0)
    first_kv = y < ny // 2

    def head_of(wide):
        return jnp.where(first_kv, wide[:, :HEAD], wide[:, HEAD:])

    def head_norm(raw, gain):
        return raw * lax.rsqrt(jnp.mean(raw * raw, axis=-1, keepdims=True) + EPSILON) * gain

    inv_rms = lax.rsqrt(ssq[...] / dim + EPSILON)
    keys = head_norm(head_of(kacc[...]), kg_ref[...]).astype(BF16)
    values = (head_of(vacc[...]) * inv_rms).astype(BF16)
    kv[0, WINDOW:] = keys
    kv[1, WINDOW:] = values

    leads = jnp.logical_and(ep == 0, c == 0)
    trails = jnp.logical_and(ep == n_ep - 1, c == CORES - 1)
    after_ep = jnp.where(c == CORES - 1, lax.rem(ep + 1, n_ep), ep)
    halo = pltpu.make_async_remote_copy(
        src_ref=kv.at[:, pl.ds(rows, WINDOW)],
        dst_ref=kv.at[:, pl.ds(0, WINDOW)],
        send_sem=halo_send,
        recv_sem=halo_recv,
        device_id=(after_ep, y * CORES + other),
        device_id_type=MESH,
    )

    @pl.when(jnp.logical_not(trails))
    def _():
        halo.start()

    @pl.when(leads)
    def _():
        kv[:, :WINDOW] = jnp.zeros((2, WINDOW, HEAD), BF16)

    gw_in.wait_recv()
    uw_in.wait_recv()

    def weight_rows(part):
        return pl.ds(pl.multiple_of(part * cols, cols), cols)

    def gate_up(part, first):
        portion = rg[part]
        gate_sum = dot(portion, gw[weight_rows(part), :])
        up_sum = dot(portion, uw[weight_rows(part), :])
        if first:
            gacc[...] = gate_sum
            uacc[...] = up_sum
        else:
            gacc[...] += gate_sum
            uacc[...] += up_sum

    gate_up(y, True)

    def attend():
        @pl.when(jnp.logical_not(leads))
        def _():
            halo.wait_recv()

        sk_in.wait_recv()
        q_idx = lax.broadcasted_iota(jnp.int32, (WINDOW, 2 * WINDOW), 0)
        k_idx = lax.broadcasted_iota(jnp.int32, (WINDOW, 2 * WINDOW), 1)
        relative = q_idx + WINDOW - k_idx
        near = jnp.logical_and(relative >= 0, relative < WINDOW)
        heads = []
        for head, acc in enumerate((q0acc, q1acc)):
            queries = head_norm(acc[...], qg_ref[...]).astype(BF16)
            sink = sk[head, 0:1, 0:1]
            blocks = []
            for block in range(rows // WINDOW):
                start = block * WINDOW
                scores = lax.dot_general(
                    queries[start : start + WINDOW],
                    kv[0, start : start + 2 * WINDOW],
                    (((1,), (1,)), ((), ())),
                    preferred_element_type=F32,
                ) * HEAD ** (-0.5)
                allowed = near
                if block == 0:
                    first_key = jnp.where(leads, WINDOW, 0)
                    allowed = jnp.logical_and(near, k_idx >= first_key)
                masked = jnp.where(allowed, scores, -jnp.inf)
                peak = jnp.maximum(jnp.max(masked, axis=-1, keepdims=True), sink)
                exponent = jnp.exp(masked - peak)
                denominator = jnp.sum(exponent, axis=-1, keepdims=True) + jnp.exp(sink - peak)
                probs = (exponent / denominator).astype(BF16)
                blocks.append(dot(probs, kv[1, start : start + 2 * WINDOW]))
            heads.append(jnp.concatenate(blocks, axis=0))
        ag[y, :rows] = jnp.concatenate(heads, axis=1).astype(BF16)

    def shared_up_gate():
        sg_in.wait_recv()
        su_in.wait_recv()
        own_toks = normed[pl.ds(pl.multiple_of(c * (toks // CORES), toks // CORES), toks // CORES)]
        parts = []
        for core in range(CORES):
            gate_pre = dot(own_toks, sgs[core])
            up_pre = dot(own_toks, sus[core])
            parts.append(jax.nn.silu(gate_pre) * up_pre)
        ag[y, rows:] = jnp.concatenate(parts, axis=1).astype(BF16)

    for distance in range(1, half_ny):
        r_ring.serve(distance)
        for part in r_ring.arrived(distance):
            gate_up(part, False)
        if distance == 1:
            attend()
            for k in range(1, nx):
                wo_leg(k, False).wait_recv()
            send_partner(
                8,
                wog.at[:, pl.ds(pl.multiple_of(c * wo_rows, wo_rows), wo_rows)],
                wog.at[:, pl.ds(pl.multiple_of(c * wo_rows, wo_rows), wo_rows)],
            )
        if distance == 2:
            shared_up_gate()

    wo_other = pl.ds(pl.multiple_of(other * wo_rows, wo_rows), wo_rows)
    wo_in = to_partner(8, wog.at[:, wo_other], wog.at[:, wo_other])

    h_ring = Ring(hg, hs_sem, hr_sem, y, ny, here, pending)
    sub_rows = slots // r_subs
    far = r_ring.arrived(half_ny)[0]
    order = []
    for sub in range(r_subs // 2):
        order += [sub, sub + r_subs // 2]
    for sub in order:
        for way in range(2):
            r_ring.serve_one(half_ny, sub, way)
        at = pl.ds(sub * sub_rows, sub_rows)
        portion = rg[far, at]
        gate_pre = gacc[at] + dot(portion, gw[weight_rows(far), :])
        up_pre = uacc[at] + dot(portion, uw[weight_rows(far), :])
        hg[y, at] = (jax.nn.silu(gate_pre) * up_pre).astype(BF16)
        h_ring.start(sub)

    dw_in.wait_recv()

    def down(part, first):
        total = dot(hg[part], dw[weight_rows(part), :])
        if first:
            oacc[...] = total
        else:
            oacc[...] += total

    down(y, True)
    for distance in range(1, half_ny):
        h_ring.serve(distance)
        for part in h_ring.arrived(distance):
            down(part, False)

    a_ring = Ring(ag, as_sem, ar_sem, y, ny, here, pending)
    for sub in range(a_ring.subs):
        a_ring.start(sub)

    far = h_ring.arrived(half_ny)[0]
    back_own = pl.ds(pl.multiple_of(ep * cap, cap), cap)
    for sub in order:
        for way in range(2):
            h_ring.serve_one(half_ny, sub, way)
        at = pl.ds(sub * sub_rows, sub_rows)
        er[at] = (oacc[at] + dot(hg[far, at], dw[weight_rows(far), :])).astype(BF16)

        def back(k, carry):
            target = lax.rem(ep + k, n_ep)
            source = pl.ds(pl.multiple_of(k * cap, cap), cap)
            for core in range(CORES):
                pltpu.make_async_remote_copy(
                    src_ref=er.at[source, pl.ds(core * mine, mine)],
                    dst_ref=ret.at[c, back_own],
                    send_sem=back_send.at[core],
                    recv_sem=back_recv.at[c],
                    device_id=(target, y * CORES + core),
                    device_id_type=MESH,
                ).start()
            return carry

        lax.fori_loop(max(1, sub * per_sub), (sub + 1) * per_sub, back, 0)
        if sub == 0:
            pltpu.make_async_copy(
                er.at[pl.ds(0, cap), own_lanes], ret.at[c, back_own], back_local
            ).start()
            send_partner(9, er.at[pl.ds(0, cap), other_lanes], ret.at[c, back_own])
    back_in = to_partner(9, er.at[pl.ds(0, cap), other_lanes], ret.at[other, back_own])

    for distance in range(1, half_ny + 1):
        a_ring.serve(distance)

    shared_rows = toks // CORES
    send_partner(10, ag.at[:, pl.ds(rows, shared_rows)], shp)
    shared_in = to_partner(10, ag.at[:, pl.ds(rows, shared_rows)], shp)
    wo_in.wait_recv()
    out = jnp.zeros((rows, cols), F32)
    for part in range(ny):
        out = out + dot(ag[part, :rows], wog[part])
    out = out.astype(BF16)
    mos[0] = jnp.where(c == 0, out[:, :mine], out[:, mine:])
    mos[1] = jnp.where(c == 0, out[:, mine:], out[:, :mine])
    send_partner(11, mos.at[1], mos.at[2])
    out_in = to_partner(11, mos.at[1], mos.at[2])

    mine_sum = jnp.zeros((shared_rows, mine), F32)
    for part in range(ny):
        mine_sum = mine_sum + dot(ag[part, rows:], sd_ref[part * 2 * HEAD : (part + 1) * 2 * HEAD, :])
    shared_in.wait_recv()
    their_sum = jnp.zeros((shared_rows, mine), F32)
    for part in range(ny):
        their_sum = their_sum + dot(shp[part], sd_ref[part * 2 * HEAD : (part + 1) * 2 * HEAD, :])
    low = jnp.where(c == 0, mine_sum, their_sum)
    high = jnp.where(c == 0, their_sum, mine_sum)
    result = jnp.concatenate([low, high], axis=0)

    weight = jnp.zeros((toks, n_ep), F32)
    for k in range(topk):
        weight = weight + jnp.where(ids_ref[:, k : k + 1] == expert_idx, rw_ref[:, k : k + 1], 0.0)
    pieces = []
    for _ in range(3):
        piece = weight.astype(BF16)
        pieces.append(piece)
        weight = weight - piece.astype(F32)
    mo_ref[own_rows, :] = mos[0]

    pltpu.make_async_copy(
        er.at[pl.ds(0, cap), own_lanes], ret.at[c, back_own], back_local
    ).wait()
    back_in.wait_recv()
    elsewhere = slots - cap
    for half in range(CORES):
        landed = ret.at[half, pl.ds(0, elsewhere)]
        pltpu.make_async_copy(landed, landed, back_recv.at[half]).wait()
    for half in range(CORES):
        mask = chosen(half)
        for piece in pieces:
            spread_weight = jnp.where(mask, dot(piece, spread), 0.0).astype(BF16)
            result = result + dot(spread_weight, ret[half])
    eo_ref[...] = result.astype(BF16)

    out_in.wait_recv()
    mo_ref[other_rows, :] = mos[2]

    sent = og.at[pl.ds(0, elsewhere)]
    pltpu.make_async_copy(sent, sent, disp_send).wait()
    for core in range(CORES):
        sent = ret.at[0, pl.ds(0, elsewhere)]
        pltpu.make_async_copy(sent, sent, back_send.at[core]).wait()
    for copy in pending:
        copy.wait_send()

    @pl.when(jnp.logical_not(trails))
    def _():
        halo.wait_send()


def shards(
    mixer_input,
    mixer_gain,
    w_query,
    w_key,
    w_value,
    query_gain,
    key_gain,
    sink_logit,
    w_output,
    expert_input,
    expert_gain,
    route_ids,
    route_weight,
    expert_gate,
    expert_up,
    expert_down,
    shared_gate,
    shared_up,
    shared_down,
):
    n_ep, n_tp = lax.axis_size("ep"), lax.axis_size("tp")
    ny, nx = n_tp // CORES, min(X_SIZE, n_ep)
    rows_all, mine = mixer_input.shape
    rows = rows_all // CORES
    toks, dim = expert_input.shape
    cols = dim // ny
    slots = 2 * toks * route_ids.shape[1] // CORES
    units = expert_gate.shape[2] * CORES
    a_rows = rows + toks // CORES
    dma = pltpu.SemaphoreType.DMA
    vmem = pl.BlockSpec(memory_space=pltpu.VMEM)
    smem = pl.BlockSpec(memory_space=pltpu.SMEM)
    hbm = pl.BlockSpec(memory_space=pl.ANY)

    def ring_sems(subs):
        return [dma((2, ny // 2, subs)), dma((2, ny // 2, subs))]

    return pl.pallas_call(
        functools.partial(kernel, n_ep, ny, nx),
        name="layer",
        out_shape=(
            jax.ShapeDtypeStruct((rows_all, mine), BF16),
            jax.ShapeDtypeStruct((toks, mine), BF16),
        ),
        in_specs=[
            vmem,
            vmem,
            hbm,
            vmem,
            vmem,
            vmem,
            vmem,
            smem,
            vmem,
            vmem,
            vmem,
            vmem,
            vmem,
            hbm,
            hbm,
            hbm,
            hbm,
            hbm,
            vmem,
        ],
        out_specs=(vmem, vmem),
        scratch_shapes=[
            pltpu.VMEM((ny, rows, cols), BF16),
            pltpu.VMEM((ny, slots, cols), BF16),
            pltpu.VMEM((ny, slots, units), BF16),
            pltpu.VMEM((ny, a_rows, 2 * HEAD), BF16),
            pltpu.VMEM((dim, units), BF16),
            pltpu.VMEM((dim, units), BF16),
            pltpu.VMEM((expert_down.shape[1], cols), BF16),
            pltpu.VMEM((2,) + w_query.shape, BF16),
            pltpu.VMEM((2,) + shared_gate.shape, BF16),
            pltpu.VMEM((2,) + shared_up.shape, BF16),
            pltpu.VMEM((ny, 2 * w_output.shape[0], cols), BF16),
            pltpu.VMEM((slots, cols), BF16),
            pltpu.VMEM((slots, cols), BF16),
            pltpu.VMEM((2, slots, mine), BF16),
            pltpu.VMEM((toks, dim), BF16),
            pltpu.VMEM((slots, units), F32),
            pltpu.VMEM((slots, units), F32),
            pltpu.VMEM((slots, cols), F32),
            pltpu.VMEM((rows, HEAD), F32),
            pltpu.VMEM((rows, HEAD), F32),
            pltpu.VMEM((rows, 2 * HEAD), F32),
            pltpu.VMEM((rows, 2 * HEAD), F32),
            pltpu.VMEM((rows, 1), F32),
            pltpu.VMEM((2, WINDOW + rows, HEAD), BF16),
            pltpu.VMEM((2, 8, 128), F32),
            pltpu.VMEM((3, rows, mine), BF16),
            pltpu.VMEM((ny, toks // CORES, 2 * HEAD), BF16),
        ]
        + ring_sems(4)
        + ring_sems(4)
        + ring_sems(4)
        + ring_sems(2)
        + [
            dma((8,)),
            dma((12,)),
            dma((12,)),
            dma(()),
            dma((4,)),
            dma((2,)),
            dma((2,)),
            dma(()),
            dma((ny - 1 + nx - 1,)),
            dma((ny - 1 + nx - 1,)),
            dma(()),
            dma(()),
        ],
        compiler_params=pltpu.CompilerParams(
            collective_id=0, has_side_effects=True, vmem_limit_bytes=56 * 1024 * 1024
        ),
    )(
        mixer_input,
        mixer_gain.reshape(1, -1),
        w_query,
        w_key,
        w_value,
        query_gain.reshape(1, -1),
        key_gain.reshape(1, -1),
        sink_logit,
        w_output,
        expert_input,
        expert_gain.reshape(1, -1),
        route_ids,
        route_weight,
        expert_gate,
        expert_up,
        expert_down,
        shared_gate,
        shared_up,
        shared_down,
    )


def solution(mesh):
    in_specs = (
        P("ep", "tp"),
        P(),
        P(None, "tp"),
        P(),
        P(),
        P(),
        P(),
        P("tp"),
        P("tp", None),
        P("ep", None),
        P(),
        P("ep", None),
        P("ep", None),
        P("ep", None, "tp"),
        P("ep", None, "tp"),
        P("ep", None, "tp"),
        P(None, "tp"),
        P(None, "tp"),
        P(None, "tp"),
    )
    out_specs = (P("ep", "tp"), P("ep", "tp"))
    return jax.shard_map(shards, mesh=mesh, in_specs=in_specs, out_specs=out_specs, check_vma=False)
```

time: 251 us -> 105 us (0.42)
  waiting for transfers between devices: 133 us -> 0 us
  Pallas kernels: 0 us -> 94.7 us
  blocking collectives: 42.6 us -> 0 us
  starting transfers between devices: 23.2 us -> 0 us
  matrix products: 18.5 us -> 0 us
  between operations: 14.9 us -> 1.31 us
  other arithmetic: 7.45 us -> 0 us
    all_gather x4 -> x0, waiting for transfers between devices: 132 us -> none  [the longest x1 49.5 us: shards(): portion = lax.all_gather(arrived, 'tp', axis=1, tiled=True)]
    pallas_call x0 -> x1, Pallas kernels: none -> 94.7 us  [shards(): pl.pallas_call(functools.partial(kernel, n_ep, ny, nx), name='layer', out...]
    all_to_all x1 -> x0, blocking collectives: 25 us -> none  [shards(): lax.all_to_all(outgoing, 'ep', split_axis=0, concat_axis=0, tiled=True)]
    dot_general x12 -> x0, matrix products: 18.5 us -> none  [the longest x1 4.18 us: shards(): jnp.dot(lax.all_gather(routed_hidden, 'tp', axis=1, tiled=True), routed_p...]
    all_gather x1 -> x0, blocking collectives: 17.6 us -> none  [shards(): lax.all_gather(shared_hidden, 'tp', axis=1, tiled=True)]
    all_to_all x2 -> x0, starting transfers between devices: 16.8 us -> none  [the longest x1 10.4 us: shards(): lax.all_to_all(expert_rows, 'ep', split_axis=0, concat_axis=0, tiled=True)]
    unnamed x35 -> x17, local copies, waits for them, and re-layouts: 1.63 us -> 8.36 us
    ppermute x2 -> x0, starting transfers between devices: 6.19 us -> none  [from_behind(): lax.ppermute(value, axis, [(source, source + steps) for source in range(f...]
  transfers between devices with their start and end apart: 8 -> 0, of which waited for: 5 -> 0; matrix products, arithmetic and copies ran while one was open for 9% -> 0% of each run, Pallas kernels for 0% -> 0%
where the time goes in v1:
time: 105 us; the launch traced here: 104 us
  Pallas kernels  94.7 us (90%)
  local copies, waits for them, and re-layouts  8.36 us (8%)
  between operations  1.31 us (1%)
    pallas_call x1, Pallas kernels, shards(): pl.pallas_call(functools.partial(kernel, n_ep, ny, nx), name='layer', out...  94.7 us
    unnamed x17, local copies, waits for them, and re-layouts  8.36 us

profile of v1, /device:TPU:1, one launch (start us, length us, event | category | flops | bytes accessed | tf_op | source)
XLA Modules:
  0.0 104.4 jit_solution(7107000283993984294)
XLA Ops:
  1.3 0.0 copy-start.3
  1.3 0.7 copy-done.3
  2.0 0.0 copy-start.4
  2.0 0.7 copy.22.ids_ref
  2.7 0.0 copy-done.4
  2.7 0.7 copy.23.rw_ref
  3.4 0.0 copy-start
  3.4 2.0 %copy.21.wq_ref = bf16[2048,64]{1,0:T(8,128)(2,1)} copy(bf16[2048,64]{0,1:T(8,128)(2,1)} %param.21) | data formatting | bytes 524288 | tf_op args[2]
  5.4 0.0 copy-done
  5.4 0.0 copy-start.1
  5.4 1.0 copy.24.sg_ref
  6.4 0.0 copy-done.1
  6.4 1.0 copy.25.su_ref
  7.5 94.7 %layer.1 = (bf16[512,128]{1,0:T(8,128)(2,1)}, bf16[128,128]{1,0:T(8,128)(2,1)}) custom-call(bf16[512,128]{1,0:T(8,128)(2,1)} %x_ref.1, f32[1,2048]{1,0:T(1,128)} %bitcast.4, bf16[2048,64]{1,0:T(8,128)(2,1)} %copy.21.wq_ref, bf16[2048,128]{1,0:T(8,128)(2,1)} %wk_ref.1, bf16[2048,128]{1,0:T(8,128)(2,1)} %wv_ref.1, f32[1,64]{1,0:T(1,128)} %bitcast.6, ...), custom_call_target="tpu_custom_call" | custom-call | tf_op jit(solution)/shard_map/layer/pallas_call | solution.py:688
  102.2 0.0 copy-start.2
  102.2 1.6 %copy.29 = bf16[512,128]{1,0:T(8,128)(2,1)} copy(bf16[512,128]{1,0:T(8,128)(2,1)} %get-tuple-element.4) | data formatting | bytes 262144
  103.8 0.0 copy-done.2
  103.8 0.6 copy.30
Async XLA Ops:
  1.3 0.7 copy-start.3
  2.0 0.7 copy-start.4
  3.4 2.0 %copy-start = (bf16[2048,64]{0,1:T(8,128)(2,1)S(1)}, bf16[2048,64]{0,1:T(8,128)(2,1)}, u32[]{:S(2)}) copy-start(bf16[2048,64]{0,1:T(8,128)(2,1)} %param.35) | copy-start | bytes 786436
  5.4 1.0 copy-start.1
  102.2 1.6 %copy-start.2 = (bf16[128,128]{1,0:T(8,128)(2,1)S(1)}, bf16[128,128]{1,0:T(8,128)(2,1)}, u32[]{:S(2)}) copy-start(bf16[128,128]{1,0:T(8,128)(2,1)} %get-tuple-element.5) | copy-start | bytes 98308

commit v2 on v1

v2 whole, which is shorter than its diff:
```python
import functools

import jax
import jax.numpy as jnp
from jax import lax
from jax.experimental import pallas as pl
from jax.experimental.pallas import tpu as pltpu
from jax.sharding import PartitionSpec as P

HEAD = 64
WINDOW = 128
EPSILON = 1e-06
CORES = 2
X_SIZE = 4
REACH = 2
F32 = jnp.float32
BF16 = jnp.bfloat16
MESH = pl.DeviceIdType.MESH


def mod(value, count):
    return lax.rem(value + count, count)


def dot(a, b):
    return jnp.dot(a, b, preferred_element_type=F32)


def dot_rows(a, b):
    return lax.dot_general(a, b, (((1,), (1,)), ((), ())), preferred_element_type=F32)


class Ring:
    def __init__(self, buf, send_sem, recv_sem, y, ny, place, pending, reach=None):
        self.buf, self.send_sem, self.recv_sem = buf, send_sem, recv_sem
        self.reach = reach
        self.y, self.ny, self.place, self.pending = y, ny, place, pending
        self.subs = send_sem.shape[2]
        self.half = ny // 2
        self.rows = buf.shape[1] // self.subs

    def carries(self, way, distance, sub):
        if self.reach is not None:
            return distance <= self.reach
        if distance < self.half:
            return True
        if distance > self.half:
            return False
        return (sub < self.subs // 2) == (way == 0)

    def copy(self, way, distance, sub):
        sign = 1 if way == 0 else -1
        part = mod(self.y - sign * (distance - 1), self.ny)
        rows = pl.ds(sub * self.rows, self.rows)
        return pltpu.make_async_remote_copy(
            src_ref=self.buf.at[part, rows],
            dst_ref=self.buf.at[part, rows],
            send_sem=self.send_sem.at[way, distance - 1, sub],
            recv_sem=self.recv_sem.at[way, distance - 1, sub],
            device_id=self.place(mod(self.y + sign, self.ny)),
            device_id_type=MESH,
        )

    def arrival(self, way, distance, sub):
        sign = 1 if way == 0 else -1
        part = mod(self.y - sign * distance, self.ny)
        rows = pl.ds(sub * self.rows, self.rows)
        return pltpu.make_async_remote_copy(
            src_ref=self.buf.at[part, rows],
            dst_ref=self.buf.at[part, rows],
            send_sem=self.send_sem.at[way, distance - 1, sub],
            recv_sem=self.recv_sem.at[way, distance - 1, sub],
            device_id=self.place(mod(self.y + sign, self.ny)),
            device_id_type=MESH,
        )

    def send(self, distance, sub, way):
        if self.carries(way, distance, sub):
            copy = self.copy(way, distance, sub)
            copy.start()
            self.pending.append(copy)

    def start(self, sub):
        for way in range(2):
            self.send(1, sub, way)

    def serve_one(self, distance, sub, way):
        if self.carries(way, distance, sub):
            self.arrival(way, distance, sub).wait_recv()
            self.send(distance + 1, sub, way)

    def serve(self, distance):
        for sub in range(self.subs):
            for way in range(2):
                self.serve_one(distance, sub, way)

    def arrived(self, distance):
        if distance < self.half:
            return [mod(self.y - distance, self.ny), mod(self.y + distance, self.ny)]
        return [mod(self.y - distance, self.ny)]


def kernel(
    n_ep,
    ny,
    nx,
    x_ref,
    gain_ref,
    wq_ref,
    wk_ref,
    wv_ref,
    qg_ref,
    kg_ref,
    sink_ref,
    wo_ref,
    ei_ref,
    eg_ref,
    ids_ref,
    rw_ref,
    gate_ref,
    up_ref,
    down_ref,
    sg_ref,
    su_ref,
    sd_ref,
    mo_ref,
    eo_ref,
    xg,
    xv,
    eiv,
    wkv,
    wvv,
    wov,
    sdv,
    rg,
    hg,
    ag,
    gw,
    uw,
    dw,
    wqs,
    sgs,
    sus,
    wog,
    og,
    er,
    ret,
    wide,
    macc,
    eov,
    normed,
    gacc,
    uacc,
    oacc,
    qacc,
    kacc,
    vacc,
    ssq,
    kv,
    sk,
    mos,
    shp,
    xs_sem,
    xr_sem,
    rs_sem,
    rr_sem,
    hs_sem,
    hr_sem,
    as_sem,
    ar_sem,
    local_sem,
    pair_send,
    pair_recv,
    disp_send,
    disp_recv,
    back_send,
    back_recv,
    back_local,
    wo_send,
    wo_recv,
    halo_send,
    halo_recv,
    out_sem,
):
    ep = lax.axis_index("ep")
    tp = lax.axis_index("tp")
    y = tp // CORES
    c = lax.rem(tp, CORES)
    other = 1 - c
    half_ny = ny // 2
    rows = x_ref.shape[0] // CORES
    toks = ei_ref.shape[0]
    dim = ei_ref.shape[1]
    cols = dim // ny
    mine = dim // (ny * CORES)
    cap = er.shape[0] // n_ep
    slots = er.shape[0]
    xi = lax.rem(ep, nx)
    pending = []
    far_parts = [mod(y + REACH + 1 + k, ny) for k in range(ny - 1 - 2 * REACH)]

    def here(place):
        return (ep, place * CORES + c)

    partner = (ep, y * CORES + other)

    own_lanes = pl.ds(pl.multiple_of(c * mine, mine), mine)
    other_lanes = pl.ds(pl.multiple_of(other * mine, mine), mine)
    own_head = pl.ds(pl.multiple_of(c * HEAD, HEAD), HEAD)
    other_head = pl.ds(pl.multiple_of(other * HEAD, HEAD), HEAD)
    own_rows = pl.ds(pl.multiple_of(c * rows, rows), rows)
    other_rows = pl.ds(pl.multiple_of(other * rows, rows), rows)
    wo_rows = wo_ref.shape[0]
    wo_piece = wo_rows // nx
    wo_src = pl.ds(pl.multiple_of(xi * wo_piece, wo_piece), wo_piece)
    wo_dst = pl.ds(pl.multiple_of(c * wo_rows + xi * wo_piece, wo_piece), wo_piece)
    wo_own = pl.ds(pl.multiple_of(c * wo_rows, wo_rows), wo_rows)
    wo_other = pl.ds(pl.multiple_of(other * wo_rows, wo_rows), wo_rows)

    def lanes_of(part):
        return pl.ds(pl.multiple_of(part * cols, cols), cols)

    def load(index, source, target):
        copy = pltpu.make_async_copy(source, target, local_sem.at[index])
        copy.start()
        return copy

    ei_in = load(0, ei_ref, eiv)
    xv_in = load(1, x_ref.at[other_rows], xv)
    x_own_in = load(2, x_ref.at[own_rows], xg.at[y, :, own_lanes])

    barrier = pltpu.get_barrier_semaphore()

    def greet(k, carry):
        target = lax.rem(ep + k, n_ep)
        for core in range(CORES):
            pl.semaphore_signal(
                barrier, inc=1, device_id=(target, y * CORES + core), device_id_type=MESH
            )
        return carry

    lax.fori_loop(1, n_ep, greet, 0)
    for k in range(1, ny):
        pl.semaphore_signal(barrier, inc=1, device_id=here(mod(y + k, ny)), device_id_type=MESH)
    pl.semaphore_signal(barrier, inc=1, device_id=partner, device_id_type=MESH)
    wov_in = load(3, wo_ref, wov)
    weights_in = [
        load(4, wq_ref, wqs.at[own_head]),
        load(5, wk_ref, wkv),
        load(6, wv_ref, wvv),
        load(7, gate_ref.at[0], gw.at[:, own_lanes]),
        load(8, up_ref.at[0], uw.at[:, own_lanes]),
        load(9, sg_ref, sgs.at[own_head]),
        load(10, su_ref, sus.at[own_head]),
        load(11, down_ref.at[0], dw.at[:, own_lanes]),
        load(12, sd_ref, sdv),
    ]
    sk[c] = jnp.full((8, 128), sink_ref[0], F32)

    topk = ids_ref.shape[0]
    expert_idx = lax.broadcasted_iota(jnp.int32, (n_ep, toks), 0)
    named = jnp.zeros((n_ep, toks), F32)
    for k in range(topk):
        named = named + jnp.where(ids_ref[k : k + 1, :] == expert_idx, 1.0, 0.0)
    t_row = lax.broadcasted_iota(jnp.int32, (toks, toks), 0)
    t_col = lax.broadcasted_iota(jnp.int32, (toks, toks), 1)
    before = jnp.where(t_row < t_col, 1.0, 0.0).astype(BF16)
    rank = dot(named.astype(BF16), before)
    rank = jnp.where(named > 0.0, rank, -1.0)
    e_row = lax.broadcasted_iota(jnp.int32, (slots, n_ep), 0)
    e_col = lax.broadcasted_iota(jnp.int32, (slots, n_ep), 1)
    spread = jnp.where(e_row // cap == e_col, 1.0, 0.0).astype(BF16)
    slot_row = lax.rem(lax.broadcasted_iota(jnp.int32, (slots, toks), 0), cap)
    rank_tall = dot(spread, rank.astype(BF16)).astype(jnp.int32) - slot_row
    pick = jnp.where(rank_tall == c * cap, 1.0, 0.0).astype(BF16)
    ei_in.wait()
    expert_float = eiv[...].astype(F32)
    squares = jnp.mean(expert_float * expert_float, axis=-1, keepdims=True)
    normed[...] = (expert_float * lax.rsqrt(squares + EPSILON) * eg_ref[...]).astype(BF16)
    og[0] = dot(pick, normed[:, lanes_of(y)]).astype(BF16)
    xv_in.wait()
    x_own_in.wait()

    pl.semaphore_wait(barrier, (n_ep - 1) * CORES + (ny - 1) + 1)

    def to_partner(index, source, target):
        return pltpu.make_async_remote_copy(
            src_ref=source,
            dst_ref=target,
            send_sem=pair_send.at[index],
            recv_sem=pair_recv.at[index],
            device_id=partner,
            device_id_type=MESH,
        )

    def send_partner(index, source, target):
        copy = to_partner(index, source, target)
        copy.start()
        pending.append(copy)

    send_partner(0, xv, xg.at[y, :, own_lanes])
    x_in = to_partner(0, xv, xg.at[y, :, other_lanes])

    r_subs = rs_sem.shape[2]
    per_sub = n_ep // r_subs

    def dispatch(block, part, sem_of):
        own = pltpu.make_async_copy(
            og.at[block, pl.ds(pl.multiple_of(ep * cap, cap), cap)],
            rg.at[part, pl.ds(0, cap)],
            disp_recv.at[sem_of(0)],
        )
        own.start()

        def send(k, carry):
            target = lax.rem(ep + n_ep - k, n_ep)
            pltpu.make_async_remote_copy(
                src_ref=og.at[block, pl.ds(pl.multiple_of(target * cap, cap), cap)],
                dst_ref=rg.at[part, pl.ds(pl.multiple_of(k * cap, cap), cap)],
                send_sem=disp_send.at[block],
                recv_sem=disp_recv.at[sem_of(k)],
                device_id=(target, tp),
                device_id_type=MESH,
            ).start()
            return carry

        lax.fori_loop(1, n_ep, send, 0)

    dispatch(0, y, lambda k: k // per_sub)

    x_ring = Ring(xg, xs_sem, xr_sem, y, ny, here, pending)
    x_in.wait_recv()
    for sub in range(x_ring.subs):
        x_ring.start(sub)

    for k, part in enumerate(far_parts):
        og[k + 1] = dot(pick, normed[:, lanes_of(part)]).astype(BF16)
        dispatch(k + 1, part, lambda _, k=k: r_subs + k)

    wov_in.wait()
    wo_self = pltpu.make_async_copy(
        wov.at[wo_src, lanes_of(y)], wog.at[y, wo_dst], local_sem.at[3]
    )
    wo_self.start()

    def wo_y(k, part):
        place = mod(y + k, ny)
        return pltpu.make_async_remote_copy(
            src_ref=wov.at[wo_src, lanes_of(place)],
            dst_ref=wog.at[part, wo_dst],
            send_sem=wo_send.at[k - 1],
            recv_sem=wo_recv.at[k - 1],
            device_id=here(place),
            device_id_type=MESH,
        )

    for k in range(1, ny):
        copy = wo_y(k, y)
        copy.start()
        pending.append(copy)
    for copy in weights_in:
        copy.wait()
    send_partner(3, wqs.at[own_head], wqs.at[own_head])
    send_partner(6, sk.at[c], sk.at[c])
    wq_in = to_partner(3, wqs.at[own_head], wqs.at[other_head])
    sk_in = to_partner(6, sk.at[c], sk.at[other])

    x_ring.serve(1)
    send_partner(1, gw.at[:, own_lanes], gw.at[:, own_lanes])
    send_partner(2, uw.at[:, own_lanes], uw.at[:, own_lanes])
    gw_in = to_partner(1, gw.at[:, own_lanes], gw.at[:, other_lanes])
    uw_in = to_partner(2, uw.at[:, own_lanes], uw.at[:, other_lanes])
    x_ring.serve(2)

    r_ring = Ring(rg, rs_sem, rr_sem, y, ny, here, pending, REACH)
    for sub in range(r_subs):
        landed = rg.at[y, pl.ds(sub * per_sub * cap, per_sub * cap)]
        pltpu.make_async_copy(landed, landed, disp_recv.at[sub]).wait()
        r_ring.start(sub)

    for k in range(1, ny):
        wo_y(k, mod(y - k, ny)).wait_recv()
    wo_self.wait()

    def wo_x(k, sender):
        place = ep - xi + lax.rem(xi + k, nx)
        piece = pl.ds(pl.multiple_of(c * wo_rows + sender * wo_piece, wo_piece), wo_piece)
        return pltpu.make_async_remote_copy(
            src_ref=wog.at[:, piece],
            dst_ref=wog.at[:, piece],
            send_sem=wo_send.at[ny - 1 + k - 1],
            recv_sem=wo_recv.at[ny - 1 + k - 1],
            device_id=(place, tp),
            device_id_type=MESH,
        )

    for k in range(1, nx):
        copy = wo_x(k, xi)
        copy.start()
        pending.append(copy)

    x_ring.serve(3)
    send_partner(4, sgs.at[own_head], sgs.at[own_head])
    send_partner(5, sus.at[own_head], sus.at[own_head])
    send_partner(7, dw.at[:, own_lanes], dw.at[:, own_lanes])
    sg_in = to_partner(4, sgs.at[own_head], sgs.at[other_head])
    su_in = to_partner(5, sus.at[own_head], sus.at[other_head])
    dw_in = to_partner(7, dw.at[:, own_lanes], dw.at[:, other_lanes])

    gw_in.wait_recv()
    uw_in.wait_recv()

    def weight_rows(part):
        return pl.ds(pl.multiple_of(part * cols, cols), cols)

    def gate_up(part, first):
        portion = rg[part]
        gate_sum = dot(portion, gw[weight_rows(part), :])
        up_sum = dot(portion, uw[weight_rows(part), :])
        if first:
            gacc[...] = gate_sum
            uacc[...] = up_sum
        else:
            gacc[...] += gate_sum
            uacc[...] += up_sum

    gate_up(y, True)

    for distance in range(1, REACH):
        r_ring.serve(distance)
    for distance in range(4, half_ny + 1):
        x_ring.serve(distance)

    wq_in.wait_recv()
    qacc[...] = jnp.zeros_like(qacc)
    kacc[...] = jnp.zeros_like(kacc)
    vacc[...] = jnp.zeros_like(vacc)
    ssq[...] = jnp.zeros_like(ssq)

    def project(part, carry):
        lanes = lanes_of(part)
        portion = xg[part].astype(F32)
        scaled = (portion * gain_ref[:, lanes]).astype(BF16)
        ssq[...] += jnp.sum(portion * portion, axis=-1, keepdims=True)
        qacc[...] += dot_rows(scaled, wqs[:, lanes])
        kacc[...] += dot(scaled, wkv[lanes, :])
        vacc[...] += dot(scaled, wvv[lanes, :])
        return carry

    lax.fori_loop(0, ny, project, 0)
    first_kv = y < ny // 2

    def head_of(both):
        return jnp.where(first_kv, both[:, :HEAD], both[:, HEAD:])

    def head_norm(raw, gain):
        return raw * lax.rsqrt(jnp.mean(raw * raw, axis=-1, keepdims=True) + EPSILON) * gain

    inv_rms = lax.rsqrt(ssq[...] / dim + EPSILON)
    keys = head_norm(head_of(kacc[...]), kg_ref[...]).astype(BF16)
    values = (head_of(vacc[...]) * inv_rms).astype(BF16)
    kv[0, WINDOW:] = keys
    kv[1, WINDOW:] = values

    leads = jnp.logical_and(ep == 0, c == 0)
    trails = jnp.logical_and(ep == n_ep - 1, c == CORES - 1)
    after_ep = jnp.where(c == CORES - 1, lax.rem(ep + 1, n_ep), ep)
    halo = pltpu.make_async_remote_copy(
        src_ref=kv.at[:, pl.ds(rows, WINDOW)],
        dst_ref=kv.at[:, pl.ds(0, WINDOW)],
        send_sem=halo_send,
        recv_sem=halo_recv,
        device_id=(after_ep, y * CORES + other),
        device_id_type=MESH,
    )

    @pl.when(jnp.logical_not(trails))
    def _():
        halo.start()

    @pl.when(leads)
    def _():
        kv[:, :WINDOW] = jnp.zeros((2, WINDOW, HEAD), BF16)

    for distance in range(1, REACH):
        for part in r_ring.arrived(distance):
            gate_up(part, False)

    sg_in.wait_recv()
    su_in.wait_recv()
    shared_rows = toks // CORES
    own_toks = normed[pl.ds(pl.multiple_of(c * shared_rows, shared_rows), shared_rows)]
    gate_pre = dot_rows(own_toks, sgs[...])
    up_pre = dot_rows(own_toks, sus[...])
    ag[y, rows:] = (jax.nn.silu(gate_pre) * up_pre).astype(BF16)

    @pl.when(jnp.logical_not(leads))
    def _():
        halo.wait_recv()

    sk_in.wait_recv()
    q_idx = lax.broadcasted_iota(jnp.int32, (WINDOW, 2 * WINDOW), 0)
    k_idx = lax.broadcasted_iota(jnp.int32, (WINDOW, 2 * WINDOW), 1)
    relative = q_idx + WINDOW - k_idx
    near = jnp.logical_and(relative >= 0, relative < WINDOW)
    heads = []
    for head in range(2):
        raw = qacc[:, head * HEAD : (head + 1) * HEAD]
        queries = head_norm(raw, qg_ref[...]).astype(BF16)
        sink = sk[head, 0:1, 0:1]
        blocks = []
        for block in range(rows // WINDOW):
            start = block * WINDOW
            scores = dot_rows(
                queries[start : start + WINDOW], kv[0, start : start + 2 * WINDOW]
            ) * HEAD ** (-0.5)
            allowed = near
            if block == 0:
                first_key = jnp.where(leads, WINDOW, 0)
                allowed = jnp.logical_and(near, k_idx >= first_key)
            masked = jnp.where(allowed, scores, -jnp.inf)
            peak = jnp.maximum(jnp.max(masked, axis=-1, keepdims=True), sink)
            exponent = jnp.exp(masked - peak)
            denominator = jnp.sum(exponent, axis=-1, keepdims=True) + jnp.exp(sink - peak)
            probs = (exponent / denominator).astype(BF16)
            blocks.append(dot(probs, kv[1, start : start + 2 * WINDOW]))
        heads.append(jnp.concatenate(blocks, axis=0))
    ag[y, :rows] = jnp.concatenate(heads, axis=1).astype(BF16)

    a_ring = Ring(ag, as_sem, ar_sem, y, ny, here, pending)
    for sub in range(a_ring.subs):
        a_ring.start(sub)
    for k in range(1, nx):
        wo_x(k, lax.rem(xi + nx - k, nx)).wait_recv()
    send_partner(8, wog.at[:, wo_own], wog.at[:, wo_own])
    wo_in = to_partner(8, wog.at[:, wo_other], wog.at[:, wo_other])

    for k, part in enumerate(far_parts):
        landed = rg.at[part]
        pltpu.make_async_copy(landed, landed, disp_recv.at[r_subs + k]).wait()
        gate_up(part, False)

    h_ring = Ring(hg, hs_sem, hr_sem, y, ny, here, pending)
    sub_rows = slots // r_subs
    for sub in range(r_subs):
        at = pl.ds(sub * sub_rows, sub_rows)
        gate_pre = gacc[at]
        up_pre = uacc[at]
        for way, part in enumerate(r_ring.arrived(REACH)):
            r_ring.serve_one(REACH, sub, way)
            portion = rg[part, at]
            gate_pre = gate_pre + dot(portion, gw[weight_rows(part), :])
            up_pre = up_pre + dot(portion, uw[weight_rows(part), :])
        hg[y, at] = (jax.nn.silu(gate_pre) * up_pre).astype(BF16)
        h_ring.start(sub)

    dw_in.wait_recv()

    def down(part, first):
        total = dot(hg[part], dw[weight_rows(part), :])
        if first:
            oacc[...] = total
        else:
            oacc[...] += total

    def out_part(part, first):
        total = dot(ag[part, :rows], wog[part])
        if first:
            macc[...] = total
        else:
            macc[...] += total

    down(y, True)
    wo_in.wait_recv()
    out_part(y, True)
    for distance in range(1, half_ny):
        h_ring.serve(distance)
        if distance == 1:
            a_ring.serve(1)
        for part in h_ring.arrived(distance):
            down(part, False)
        if distance == 1:
            for part in a_ring.arrived(1):
                out_part(part, False)
    a_ring.serve(2)

    order = []
    for sub in range(r_subs // 2):
        order += [sub, sub + r_subs // 2]
    last = h_ring.arrived(half_ny)[0]
    back_own = pl.ds(pl.multiple_of(ep * cap, cap), cap)
    for sub in order:
        for way in range(2):
            h_ring.serve_one(half_ny, sub, way)
        at = pl.ds(sub * sub_rows, sub_rows)
        er[at] = (oacc[at] + dot(hg[last, at], dw[weight_rows(last), :])).astype(BF16)

        def back(k, carry):
            target = lax.rem(ep + k, n_ep)
            source = pl.ds(pl.multiple_of(k * cap, cap), cap)
            for core in range(CORES):
                pltpu.make_async_remote_copy(
                    src_ref=er.at[source, pl.ds(core * mine, mine)],
                    dst_ref=ret.at[c, back_own],
                    send_sem=back_send.at[core],
                    recv_sem=back_recv.at[c],
                    device_id=(target, y * CORES + core),
                    device_id_type=MESH,
                ).start()
            return carry

        lax.fori_loop(max(1, sub * per_sub), (sub + 1) * per_sub, back, 0)
        if sub == 0:
            back_mine = pltpu.make_async_copy(
                er.at[pl.ds(0, cap), own_lanes], ret.at[c, back_own], back_local
            )
            back_mine.start()
            send_partner(9, er.at[pl.ds(0, cap), other_lanes], ret.at[c, back_own])
    back_in = to_partner(9, er.at[pl.ds(0, cap), other_lanes], ret.at[other, back_own])

    for part in a_ring.arrived(2):
        out_part(part, False)
    for distance in range(3, half_ny):
        a_ring.serve(distance)
        for part in a_ring.arrived(distance):
            out_part(part, False)

    weight = jnp.zeros((n_ep, toks), F32)
    for k in range(topk):
        weight = weight + jnp.where(ids_ref[k : k + 1, :] == expert_idx, rw_ref[k : k + 1, :], 0.0)
    n_pieces = wide.shape[0] // CORES
    for index in range(n_pieces):
        piece = weight.astype(BF16)
        weight = weight - piece.astype(F32)
        tall = dot(spread, piece)
        for half in range(CORES):
            wide[half * n_pieces + index] = jnp.transpose(
                jnp.where(rank_tall == half * cap, tall, 0.0)
            ).astype(BF16)

    a_ring.serve(half_ny)
    out_part(a_ring.arrived(half_ny)[0], False)
    send_partner(10, ag.at[:, pl.ds(rows, shared_rows)], shp)
    shared_in = to_partner(10, ag.at[:, pl.ds(rows, shared_rows)], shp)
    out = macc[...].astype(BF16)
    mos[0] = jnp.where(c == 0, out[:, :mine], out[:, mine:])
    mos[1] = jnp.where(c == 0, out[:, mine:], out[:, :mine])
    send_partner(11, mos.at[1], mos.at[2])
    out_in = to_partner(11, mos.at[1], mos.at[2])
    mo_first = pltpu.make_async_copy(mos.at[0], mo_ref.at[own_rows], out_sem.at[0])
    mo_first.start()
    mine_sum = jnp.zeros((shared_rows, mine), F32)
    for part in range(ny):
        mine_sum = mine_sum + dot(ag[part, rows:], sdv[part * 2 * HEAD : (part + 1) * 2 * HEAD, :])
    shared_in.wait_recv()
    their_sum = jnp.zeros((shared_rows, mine), F32)
    for part in range(ny):
        their_sum = their_sum + dot(shp[part], sdv[part * 2 * HEAD : (part + 1) * 2 * HEAD, :])
    low = jnp.where(c == 0, mine_sum, their_sum)
    high = jnp.where(c == 0, their_sum, mine_sum)
    result = jnp.concatenate([low, high], axis=0)

    back_mine.wait()
    back_in.wait_recv()
    elsewhere = slots - cap
    for half in range(CORES):
        landed = ret.at[half, pl.ds(0, elsewhere)]
        pltpu.make_async_copy(landed, landed, back_recv.at[half]).wait()
    for half in range(CORES):
        for index in range(n_pieces):
            result = result + dot(wide[half * n_pieces + index], ret[half])
    eov[...] = result.astype(BF16)
    eo_out = pltpu.make_async_copy(eov, eo_ref, out_sem.at[1])
    eo_out.start()
    out_in.wait_recv()
    mo_second = pltpu.make_async_copy(mos.at[2], mo_ref.at[other_rows], out_sem.at[2])
    mo_second.start()

    for block in range(len(far_parts) + 1):
        sent = og.at[block, pl.ds(0, elsewhere)]
        pltpu.make_async_copy(sent, sent, disp_send.at[block]).wait()
    for core in range(CORES):
        sent = ret.at[0, pl.ds(0, elsewhere)]
        pltpu.make_async_copy(sent, sent, back_send.at[core]).wait()
    for copy in pending:
        copy.wait_send()

    @pl.when(jnp.logical_not(trails))
    def _():
        halo.wait_send()

    mo_first.wait()
    eo_out.wait()
    mo_second.wait()


def shards(
    mixer_input,
    mixer_gain,
    w_query,
    w_key,
    w_value,
    query_gain,
    key_gain,
    sink_logit,
    w_output,
    expert_input,
    expert_gain,
    route_ids,
    route_weight,
    expert_gate,
    expert_up,
    expert_down,
    shared_gate,
    shared_up,
    shared_down,
):
    n_ep, n_tp = lax.axis_size("ep"), lax.axis_size("tp")
    ny, nx = n_tp // CORES, min(X_SIZE, n_ep)
    rows_all, mine = mixer_input.shape
    rows = rows_all // CORES
    toks, dim = expert_input.shape
    cols = dim // ny
    slots = 2 * toks * route_ids.shape[1] // CORES
    units = expert_gate.shape[2] * CORES
    a_rows = rows + toks // CORES
    dma = pltpu.SemaphoreType.DMA
    vmem = pl.BlockSpec(memory_space=pltpu.VMEM)
    smem = pl.BlockSpec(memory_space=pltpu.SMEM)
    hbm = pl.BlockSpec(memory_space=pl.ANY)

    def ring_sems(subs):
        return [dma((2, ny // 2, subs)), dma((2, ny // 2, subs))]

    return pl.pallas_call(
        functools.partial(kernel, n_ep, ny, nx),
        name="layer",
        out_shape=(
            jax.ShapeDtypeStruct((rows_all, mine), BF16),
            jax.ShapeDtypeStruct((toks, mine), BF16),
        ),
        in_specs=[
            hbm,
            vmem,
            hbm,
            hbm,
            hbm,
            vmem,
            vmem,
            smem,
            hbm,
            hbm,
            vmem,
            vmem,
            vmem,
            hbm,
            hbm,
            hbm,
            hbm,
            hbm,
            hbm,
        ],
        out_specs=(hbm, hbm),
        scratch_shapes=[
            pltpu.VMEM((ny, rows, cols), BF16),
            pltpu.VMEM((rows, mine), BF16),
            pltpu.VMEM((toks, dim), BF16),
            pltpu.VMEM(w_key.shape, BF16),
            pltpu.VMEM(w_value.shape, BF16),
            pltpu.VMEM(w_output.shape, BF16),
            pltpu.VMEM(shared_down.shape, BF16),
            pltpu.VMEM((ny, slots, cols), BF16),
            pltpu.VMEM((ny, slots, units), BF16),
            pltpu.VMEM((ny, a_rows, 2 * HEAD), BF16),
            pltpu.VMEM((dim, units), BF16),
            pltpu.VMEM((dim, units), BF16),
            pltpu.VMEM((expert_down.shape[1], cols), BF16),
            pltpu.VMEM((2 * HEAD, dim), BF16),
            pltpu.VMEM((2 * HEAD, dim), BF16),
            pltpu.VMEM((2 * HEAD, dim), BF16),
            pltpu.VMEM((ny, 2 * w_output.shape[0], cols), BF16),
            pltpu.VMEM((ny - 2 * REACH, slots, cols), BF16),
            pltpu.VMEM((slots, cols), BF16),
            pltpu.VMEM((2, slots, mine), BF16),
            pltpu.VMEM((6, toks, slots), BF16),
            pltpu.VMEM((rows, cols), F32),
            pltpu.VMEM((toks, mine), BF16),
            pltpu.VMEM((toks, dim), BF16),
            pltpu.VMEM((slots, units), F32),
            pltpu.VMEM((slots, units), F32),
            pltpu.VMEM((slots, cols), F32),
            pltpu.VMEM((rows, 2 * HEAD), F32),
            pltpu.VMEM((rows, 2 * HEAD), F32),
            pltpu.VMEM((rows, 2 * HEAD), F32),
            pltpu.VMEM((rows, 1), F32),
            pltpu.VMEM((2, WINDOW + rows, HEAD), BF16),
            pltpu.VMEM((2, 8, 128), F32),
            pltpu.VMEM((3, rows, mine), BF16),
            pltpu.VMEM((ny, toks // CORES, 2 * HEAD), BF16),
        ]
        + ring_sems(4)
        + ring_sems(4)
        + ring_sems(4)
        + ring_sems(2)
        + [
            dma((13,)),
            dma((12,)),
            dma((12,)),
            dma((ny - 2 * REACH,)),
            dma((4 + ny - 1 - 2 * REACH,)),
            dma((2,)),
            dma((2,)),
            dma(()),
            dma((ny - 1 + nx - 1,)),
            dma((ny - 1 + nx - 1,)),
            dma(()),
            dma(()),
            dma((3,)),
        ],
        compiler_params=pltpu.CompilerParams(
            collective_id=0, has_side_effects=True, vmem_limit_bytes=56 * 1024 * 1024
        ),
    )(
        mixer_input,
        mixer_gain.reshape(1, -1),
        w_query.T,
        w_key,
        w_value,
        query_gain.reshape(1, -1),
        key_gain.reshape(1, -1),
        sink_logit,
        w_output,
        expert_input,
        expert_gain.reshape(1, -1),
        route_ids.T,
        route_weight.T,
        expert_gate,
        expert_up,
        expert_down,
        shared_gate.T,
        shared_up.T,
        shared_down,
    )


def solution(mesh):
    in_specs = (
        P("ep", "tp"),
        P(),
        P(None, "tp"),
        P(),
        P(),
        P(),
        P(),
        P("tp"),
        P("tp", None),
        P("ep", None),
        P(),
        P("ep", None),
        P("ep", None),
        P("ep", None, "tp"),
        P("ep", None, "tp"),
        P("ep", None, "tp"),
        P(None, "tp"),
        P(None, "tp"),
        P(None, "tp"),
    )
    out_specs = (P("ep", "tp"), P("ep", "tp"))
    return jax.shard_map(shards, mesh=mesh, in_specs=in_specs, out_specs=out_specs, check_vma=False)
```

time: 105 us -> 84.2 us (0.80)
  Pallas kernels: 94.7 us -> 80.5 us
  local copies, waits for them, and re-layouts: 8.36 us -> 2.19 us
    pallas_call x1, Pallas kernels: 94.7 us -> 80.5 us  [shards(): pl.pallas_call(functools.partial(kernel, n_ep, ny, nx), name='layer', out...]
    unnamed x17 -> x4, local copies, waits for them, and re-layouts: 8.36 us -> 2.19 us
where the time goes in v2:
time: 84.2 us; the launch traced here: 84 us
  Pallas kernels  80.5 us (96%)
  local copies, waits for them, and re-layouts  2.19 us (3%)
  between operations  1.3 us (2%)
    pallas_call x1, Pallas kernels, shards(): pl.pallas_call(functools.partial(kernel, n_ep, ny, nx), name='layer', out...  80.5 us
    unnamed x4, local copies, waits for them, and re-layouts  2.19 us

profile of v2, /device:TPU:1, one launch (start us, length us, event | category | flops | bytes accessed | tf_op | source)
XLA Modules:
  0.0 84.0 jit_solution(4411197585035203548)
XLA Ops:
  1.3 80.5 %layer.1 = (bf16[512,128]{1,0:T(8,128)(2,1)}, bf16[128,128]{1,0:T(8,128)(2,1)}) custom-call(bf16[512,128]{1,0:T(8,128)(2,1)} %x_ref.1, f32[1,2048]{1,0:T(1,128)} %bitcast.12, bf16[64,2048]{1,0:T(8,128)(2,1)} %bitcast.9, bf16[2048,128]{1,0:T(8,128)(2,1)} %wk_ref.1, bf16[2048,128]{1,0:T(8,128)(2,1)} %wv_ref.1, f32[1,64]{1,0:T(1,128)} %bitcast.16, ...), custom_call_target="tpu_custom_call" | custom-call | tf_op jit(solution)/shard_map/layer/pallas_call | solution.py:735
  81.8 0.0 copy-start
  81.8 1.6 %copy.24 = bf16[512,128]{1,0:T(8,128)(2,1)} copy(bf16[512,128]{1,0:T(8,128)(2,1)} %get-tuple-element.4) | data formatting | bytes 262144
  83.4 0.0 copy-done
  83.4 0.6 copy.25
Async XLA Ops:
  81.8 1.6 %copy-start = (bf16[128,128]{1,0:T(8,128)(2,1)S(1)}, bf16[128,128]{1,0:T(8,128)(2,1)}, u32[]{:S(2)}) copy-start(bf16[128,128]{1,0:T(8,128)(2,1)} %get-tuple-element.5) | copy-start | bytes 98308

commit v3 on v2

--- a/solution.py
+++ b/solution.py
@@ -13,6 +13,8 @@
 CORES = 2
 X_SIZE = 4
 REACH = 2
+SUBS = 4
+ORDER = (0, 3, 1, 2)
 F32 = jnp.float32
 BF16 = jnp.bfloat16
 MESH = pl.DeviceIdType.MESH
@@ -31,13 +33,12 @@
 
 
 class Ring:
-    def __init__(self, buf, send_sem, recv_sem, y, ny, place, pending, reach=None):
+    def __init__(self, buf, send_sem, recv_sem, y, ny, place, subs, reach=None):
         self.buf, self.send_sem, self.recv_sem = buf, send_sem, recv_sem
-        self.reach = reach
-        self.y, self.ny, self.place, self.pending = y, ny, place, pending
-        self.subs = send_sem.shape[2]
+        self.y, self.ny, self.place = y, ny, place
+        self.subs, self.reach = subs, reach
         self.half = ny // 2
-        self.rows = buf.shape[1] // self.subs
+        self.rows = buf.shape[1] // subs
 
     def carries(self, way, distance, sub):
         if self.reach is not None:
@@ -48,37 +49,25 @@
             return False
         return (sub < self.subs // 2) == (way == 0)
 
-    def copy(self, way, distance, sub):
+    def copy(self, way, distance, sub, origin):
         sign = 1 if way == 0 else -1
-        part = mod(self.y - sign * (distance - 1), self.ny)
+        part = mod(self.y - sign * origin, self.ny)
         rows = pl.ds(sub * self.rows, self.rows)
+        index = (distance - 1) * self.subs * 2 + sub * 2 + way
+        if self.reach is None and distance == self.half:
+            index = (distance - 1) * self.subs * 2 + sub
         return pltpu.make_async_remote_copy(
             src_ref=self.buf.at[part, rows],
             dst_ref=self.buf.at[part, rows],
-            send_sem=self.send_sem.at[way, distance - 1, sub],
-            recv_sem=self.recv_sem.at[way, distance - 1, sub],
+            send_sem=self.send_sem,
+            recv_sem=self.recv_sem.at[index],
             device_id=self.place(mod(self.y + sign, self.ny)),
             device_id_type=MESH,
         )
 
-    def arrival(self, way, distance, sub):
-        sign = 1 if way == 0 else -1
-        part = mod(self.y - sign * distance, self.ny)
-        rows = pl.ds(sub * self.rows, self.rows)
-        return pltpu.make_async_remote_copy(
-            src_ref=self.buf.at[part, rows],
-            dst_ref=self.buf.at[part, rows],
-            send_sem=self.send_sem.at[way, distance - 1, sub],
-            recv_sem=self.recv_sem.at[way, distance - 1, sub],
-            device_id=self.place(mod(self.y + sign, self.ny)),
-            device_id_type=MESH,
-        )
-
     def send(self, distance, sub, way):
         if self.carries(way, distance, sub):
-            copy = self.copy(way, distance, sub)
-            copy.start()
-            self.pending.append(copy)
+            self.copy(way, distance, sub, distance - 1).start()
 
     def start(self, sub):
         for way in range(2):
@@ -86,11 +75,11 @@
 
     def serve_one(self, distance, sub, way):
         if self.carries(way, distance, sub):
-            self.arrival(way, distance, sub).wait_recv()
+            self.copy(way, distance, sub, distance).wait_recv()
             self.send(distance + 1, sub, way)
 
-    def serve(self, distance):
-        for sub in range(self.subs):
+    def serve(self, distance, order=None):
+        for sub in order or range(self.subs):
             for way in range(2):
                 self.serve_one(distance, sub, way)
 
@@ -98,6 +87,11 @@
         if distance < self.half:
             return [mod(self.y - distance, self.ny), mod(self.y + distance, self.ny)]
         return [mod(self.y - distance, self.ny)]
+
+    def finish(self):
+        count = self.ny - 1 if self.reach is None else 2 * self.reach
+        sent = self.buf.at[pl.ds(0, count)]
+        pltpu.make_async_copy(sent, sent, self.send_sem).wait()
 
 
 def kernel(
@@ -105,18 +99,18 @@
     ny,
     nx,
     x_ref,
-    gain_ref,
+    gain_in,
     wq_ref,
     wk_ref,
     wv_ref,
-    qg_ref,
-    kg_ref,
-    sink_ref,
+    qg_in,
+    kg_in,
+    sink_in,
     wo_ref,
     ei_ref,
-    eg_ref,
-    ids_ref,
-    rw_ref,
+    eg_in,
+    ids_in,
+    rw_in,
     gate_ref,
     up_ref,
     down_ref,
@@ -126,6 +120,13 @@
     mo_ref,
     eo_ref,
     xg,
+    gain_ref,
+    qg_ref,
+    kg_ref,
+    sink_ref,
+    eg_ref,
+    ids_ref,
+    rw_ref,
     xv,
     eiv,
     wkv,
@@ -149,8 +150,6 @@
     macc,
     eov,
     normed,
-    gacc,
-    uacc,
     oacc,
     qacc,
     kacc,
@@ -225,9 +224,13 @@
         copy.start()
         return copy
 
+    ids_load = load(13, ids_in, ids_ref)
     ei_in = load(0, ei_ref, eiv)
+    eg_load = load(14, eg_in, eg_ref)
     xv_in = load(1, x_ref.at[other_rows], xv)
     x_own_in = load(2, x_ref.at[own_rows], xg.at[y, :, own_lanes])
+    wov_in = load(3, wo_ref, wov)
+    sink_load = load(19, sink_in, sink_ref)
 
     barrier = pltpu.get_barrier_semaphore()
 
@@ -243,7 +246,12 @@
     for k in range(1, ny):
         pl.semaphore_signal(barrier, inc=1, device_id=here(mod(y + k, ny)), device_id_type=MESH)
     pl.semaphore_signal(barrier, inc=1, device_id=partner, device_id_type=MESH)
-    wov_in = load(3, wo_ref, wov)
+    small = [
+        load(15, rw_in, rw_ref),
+        load(16, gain_in, gain_ref),
+        load(17, qg_in, qg_ref),
+        load(18, kg_in, kg_ref),
+    ]
     weights_in = [
         load(4, wq_ref, wqs.at[own_head]),
         load(5, wk_ref, wkv),
@@ -255,8 +263,10 @@
         load(11, down_ref.at[0], dw.at[:, own_lanes]),
         load(12, sd_ref, sdv),
     ]
+    sink_load.wait()
     sk[c] = jnp.full((8, 128), sink_ref[0], F32)
 
+    ids_load.wait()
     topk = ids_ref.shape[0]
     expert_idx = lax.broadcasted_iota(jnp.int32, (n_ep, toks), 0)
     named = jnp.zeros((n_ep, toks), F32)
@@ -274,6 +284,7 @@
     rank_tall = dot(spread, rank.astype(BF16)).astype(jnp.int32) - slot_row
     pick = jnp.where(rank_tall == c * cap, 1.0, 0.0).astype(BF16)
     ei_in.wait()
+    eg_load.wait()
     expert_float = eiv[...].astype(F32)
     squares = jnp.mean(expert_float * expert_float, axis=-1, keepdims=True)
     normed[...] = (expert_float * lax.rsqrt(squares + EPSILON) * eg_ref[...]).astype(BF16)
@@ -301,42 +312,6 @@
     send_partner(0, xv, xg.at[y, :, own_lanes])
     x_in = to_partner(0, xv, xg.at[y, :, other_lanes])
 
-    r_subs = rs_sem.shape[2]
-    per_sub = n_ep // r_subs
-
-    def dispatch(block, part, sem_of):
-        own = pltpu.make_async_copy(
-            og.at[block, pl.ds(pl.multiple_of(ep * cap, cap), cap)],
-            rg.at[part, pl.ds(0, cap)],
-            disp_recv.at[sem_of(0)],
-        )
-        own.start()
-
-        def send(k, carry):
-            target = lax.rem(ep + n_ep - k, n_ep)
-            pltpu.make_async_remote_copy(
-                src_ref=og.at[block, pl.ds(pl.multiple_of(target * cap, cap), cap)],
-                dst_ref=rg.at[part, pl.ds(pl.multiple_of(k * cap, cap), cap)],
-                send_sem=disp_send.at[block],
-                recv_sem=disp_recv.at[sem_of(k)],
-                device_id=(target, tp),
-                device_id_type=MESH,
-            ).start()
-            return carry
-
-        lax.fori_loop(1, n_ep, send, 0)
-
-    dispatch(0, y, lambda k: k // per_sub)
-
-    x_ring = Ring(xg, xs_sem, xr_sem, y, ny, here, pending)
-    x_in.wait_recv()
-    for sub in range(x_ring.subs):
-        x_ring.start(sub)
-
-    for k, part in enumerate(far_parts):
-        og[k + 1] = dot(pick, normed[:, lanes_of(part)]).astype(BF16)
-        dispatch(k + 1, part, lambda _, k=k: r_subs + k)
-
     wov_in.wait()
     wo_self = pltpu.make_async_copy(
         wov.at[wo_src, lanes_of(y)], wog.at[y, wo_dst], local_sem.at[3]
@@ -348,17 +323,54 @@
         return pltpu.make_async_remote_copy(
             src_ref=wov.at[wo_src, lanes_of(place)],
             dst_ref=wog.at[part, wo_dst],
-            send_sem=wo_send.at[k - 1],
-            recv_sem=wo_recv.at[k - 1],
+            send_sem=wo_send.at[0],
+            recv_sem=wo_recv.at[0],
             device_id=here(place),
             device_id_type=MESH,
         )
 
     for k in range(1, ny):
-        copy = wo_y(k, y)
-        copy.start()
-        pending.append(copy)
-    for copy in weights_in:
+        wo_y(k, y).start()
+    r_subs = SUBS
+    sub_rows = slots // r_subs
+    per_sub = n_ep // r_subs
+
+    def dispatch(blocks, parts, base):
+        for block, part in zip(blocks, parts):
+            pltpu.make_async_copy(
+                og.at[block, pl.ds(pl.multiple_of(ep * cap, cap), cap)],
+                rg.at[part, pl.ds(0, cap)],
+                disp_recv.at[base],
+            ).start()
+
+        for sub in ORDER:
+
+            def send(k, carry, sub=sub):
+                target = lax.rem(ep + n_ep - k, n_ep)
+                for block, part in zip(blocks, parts):
+                    pltpu.make_async_remote_copy(
+                        src_ref=og.at[block, pl.ds(pl.multiple_of(target * cap, cap), cap)],
+                        dst_ref=rg.at[part, pl.ds(pl.multiple_of(k * cap, cap), cap)],
+                        send_sem=disp_send.at[block],
+                        recv_sem=disp_recv.at[base + sub],
+                        device_id=(target, tp),
+                        device_id_type=MESH,
+                    ).start()
+                return carry
+
+            lax.fori_loop(max(1, sub * per_sub), (sub + 1) * per_sub, send, 0)
+
+    dispatch([0], [y], 0)
+
+    x_ring = Ring(xg, xs_sem, xr_sem, y, ny, here, 4)
+    x_in.wait_recv()
+    for sub in range(x_ring.subs):
+        x_ring.start(sub)
+
+    for k, part in enumerate(far_parts):
+        og[k + 1] = dot(pick, normed[:, lanes_of(part)]).astype(BF16)
+
+    for copy in weights_in + small:
         copy.wait()
     send_partner(3, wqs.at[own_head], wqs.at[own_head])
     send_partner(6, sk.at[c], sk.at[c])
@@ -366,20 +378,29 @@
     sk_in = to_partner(6, sk.at[c], sk.at[other])
 
     x_ring.serve(1)
+
+    dispatch(range(1, len(far_parts) + 1), far_parts, r_subs)
     send_partner(1, gw.at[:, own_lanes], gw.at[:, own_lanes])
     send_partner(2, uw.at[:, own_lanes], uw.at[:, own_lanes])
     gw_in = to_partner(1, gw.at[:, own_lanes], gw.at[:, other_lanes])
     uw_in = to_partner(2, uw.at[:, own_lanes], uw.at[:, other_lanes])
-    x_ring.serve(2)
-
-    r_ring = Ring(rg, rs_sem, rr_sem, y, ny, here, pending, REACH)
-    for sub in range(r_subs):
+
+    r_ring = Ring(rg, rs_sem, rr_sem, y, ny, here, r_subs, REACH)
+
+    def r_start(sub):
         landed = rg.at[y, pl.ds(sub * per_sub * cap, per_sub * cap)]
         pltpu.make_async_copy(landed, landed, disp_recv.at[sub]).wait()
         r_ring.start(sub)
 
-    for k in range(1, ny):
-        wo_y(k, mod(y - k, ny)).wait_recv()
+    r_start(ORDER[0])
+
+    x_ring.serve(2)
+
+    for sub in ORDER[1:]:
+        r_start(sub)
+
+    wo_y_bytes = og.at[0, pl.ds(0, (ny - 1) * wo_piece)]
+    pltpu.make_async_copy(wo_y_bytes, wo_y_bytes, wo_recv.at[0]).wait()
     wo_self.wait()
 
     def wo_x(k, sender):
@@ -388,16 +409,15 @@
         return pltpu.make_async_remote_copy(
             src_ref=wog.at[:, piece],
             dst_ref=wog.at[:, piece],
-            send_sem=wo_send.at[ny - 1 + k - 1],
-            recv_sem=wo_recv.at[ny - 1 + k - 1],
+            send_sem=wo_send.at[1],
+            recv_sem=wo_recv.at[1],
             device_id=(place, tp),
             device_id_type=MESH,
         )
 
+    wo_x_bytes = wog.at[:, pl.ds(0, (nx - 1) * wo_piece)]
     for k in range(1, nx):
-        copy = wo_x(k, xi)
-        copy.start()
-        pending.append(copy)
+        wo_x(k, xi).start()
 
     x_ring.serve(3)
     send_partner(4, sgs.at[own_head], sgs.at[own_head])
@@ -407,27 +427,35 @@
     su_in = to_partner(5, sus.at[own_head], sus.at[other_head])
     dw_in = to_partner(7, dw.at[:, own_lanes], dw.at[:, other_lanes])
 
+    for distance in range(1, REACH):
+        r_ring.serve(distance, ORDER)
+    def weight_rows(part):
+        return pl.ds(pl.multiple_of(part * cols, cols), cols)
+
+    h_ring = Ring(hg, hs_sem, hr_sem, y, ny, here, r_subs)
+    near_parts = [y]
+    for distance in range(1, REACH + 1):
+        near_parts += r_ring.arrived(distance)
+
+    def hidden(sub):
+        for way in range(2):
+            r_ring.serve_one(REACH, sub, way)
+        landed = rg.at[pl.ds(0, len(far_parts)), pl.ds(0, sub_rows)]
+        pltpu.make_async_copy(landed, landed, disp_recv.at[r_subs + sub]).wait()
+        at = pl.ds(sub * sub_rows, sub_rows)
+        gate_pre = jnp.zeros((sub_rows, gw.shape[1]), F32)
+        up_pre = jnp.zeros((sub_rows, uw.shape[1]), F32)
+        for part in near_parts + far_parts:
+            portion = rg[part, at]
+            gate_pre = gate_pre + dot(portion, gw[weight_rows(part), :])
+            up_pre = up_pre + dot(portion, uw[weight_rows(part), :])
+        hg[y, at] = (jax.nn.silu(gate_pre) * up_pre).astype(BF16)
+        h_ring.start(sub)
+
     gw_in.wait_recv()
     uw_in.wait_recv()
-
-    def weight_rows(part):
-        return pl.ds(pl.multiple_of(part * cols, cols), cols)
-
-    def gate_up(part, first):
-        portion = rg[part]
-        gate_sum = dot(portion, gw[weight_rows(part), :])
-        up_sum = dot(portion, uw[weight_rows(part), :])
-        if first:
-            gacc[...] = gate_sum
-            uacc[...] = up_sum
-        else:
-            gacc[...] += gate_sum
-            uacc[...] += up_sum
-
-    gate_up(y, True)
-
-    for distance in range(1, REACH):
-        r_ring.serve(distance)
+    hidden(ORDER[0])
+
     for distance in range(4, half_ny + 1):
         x_ring.serve(distance)
 
@@ -447,7 +475,11 @@
         vacc[...] += dot(scaled, wvv[lanes, :])
         return carry
 
-    lax.fori_loop(0, ny, project, 0)
+    lax.fori_loop(0, ny // 2, project, 0)
+
+    hidden(ORDER[1])
+
+    lax.fori_loop(ny // 2, ny, project, 0)
     first_kv = y < ny // 2
 
     def head_of(both):
@@ -482,9 +514,8 @@
     def _():
         kv[:, :WINDOW] = jnp.zeros((2, WINDOW, HEAD), BF16)
 
-    for distance in range(1, REACH):
-        for part in r_ring.arrived(distance):
-            gate_up(part, False)
+    hidden(ORDER[2])
+    h_ring.serve(1, ORDER[:2])
 
     sg_in.wait_recv()
     su_in.wait_recv()
@@ -494,74 +525,54 @@
     up_pre = dot_rows(own_toks, sus[...])
     ag[y, rows:] = (jax.nn.silu(gate_pre) * up_pre).astype(BF16)
 
-    @pl.when(jnp.logical_not(leads))
-    def _():
-        halo.wait_recv()
-
-    sk_in.wait_recv()
     q_idx = lax.broadcasted_iota(jnp.int32, (WINDOW, 2 * WINDOW), 0)
     k_idx = lax.broadcasted_iota(jnp.int32, (WINDOW, 2 * WINDOW), 1)
     relative = q_idx + WINDOW - k_idx
     near = jnp.logical_and(relative >= 0, relative < WINDOW)
-    heads = []
-    for head in range(2):
-        raw = qacc[:, head * HEAD : (head + 1) * HEAD]
-        queries = head_norm(raw, qg_ref[...]).astype(BF16)
-        sink = sk[head, 0:1, 0:1]
-        blocks = []
-        for block in range(rows // WINDOW):
-            start = block * WINDOW
-            scores = dot_rows(
-                queries[start : start + WINDOW], kv[0, start : start + 2 * WINDOW]
-            ) * HEAD ** (-0.5)
-            allowed = near
-            if block == 0:
-                first_key = jnp.where(leads, WINDOW, 0)
-                allowed = jnp.logical_and(near, k_idx >= first_key)
+    first_key = jnp.where(leads, WINDOW, 0)
+
+    @pl.when(jnp.logical_not(leads))
+    def _():
+        halo.wait_recv()
+
+    sk_in.wait_recv()
+
+    def attend(block):
+        start = block * WINDOW
+        allowed = near
+        if block == 0:
+            allowed = jnp.logical_and(near, k_idx >= first_key)
+        heads = []
+        for head in range(2):
+            raw = qacc[start : start + WINDOW, head * HEAD : (head + 1) * HEAD]
+            queries = head_norm(raw, qg_ref[...]).astype(BF16)
+            sink = sk[head, 0:1, 0:1]
+            scores = dot_rows(queries, kv[0, start : start + 2 * WINDOW]) * HEAD ** (-0.5)
             masked = jnp.where(allowed, scores, -jnp.inf)
             peak = jnp.maximum(jnp.max(masked, axis=-1, keepdims=True), sink)
             exponent = jnp.exp(masked - peak)
             denominator = jnp.sum(exponent, axis=-1, keepdims=True) + jnp.exp(sink - peak)
             probs = (exponent / denominator).astype(BF16)
-            blocks.append(dot(probs, kv[1, start : start + 2 * WINDOW]))
-        heads.append(jnp.concatenate(blocks, axis=0))
-    ag[y, :rows] = jnp.concatenate(heads, axis=1).astype(BF16)
-
-    a_ring = Ring(ag, as_sem, ar_sem, y, ny, here, pending)
+            heads.append(dot(probs, kv[1, start : start + 2 * WINDOW]))
+        ag[y, start : start + WINDOW] = jnp.concatenate(heads, axis=1).astype(BF16)
+
+    for block in range(rows // WINDOW):
+        attend(block)
+    hidden(ORDER[3])
+
+    h_ring.serve(1, ORDER[2:3])
+    h_ring.serve(2, ORDER[:2])
+    h_ring.serve(1, ORDER[3:])
+    h_ring.serve(2, ORDER[2:])
+
+    a_ring = Ring(ag, as_sem, ar_sem, y, ny, here, 2)
     for sub in range(a_ring.subs):
         a_ring.start(sub)
-    for k in range(1, nx):
-        wo_x(k, lax.rem(xi + nx - k, nx)).wait_recv()
+
+    pltpu.make_async_copy(wo_x_bytes, wo_x_bytes, wo_recv.at[1]).wait()
     send_partner(8, wog.at[:, wo_own], wog.at[:, wo_own])
     wo_in = to_partner(8, wog.at[:, wo_other], wog.at[:, wo_other])
-
-    for k, part in enumerate(far_parts):
-        landed = rg.at[part]
-        pltpu.make_async_copy(landed, landed, disp_recv.at[r_subs + k]).wait()
-        gate_up(part, False)
-
-    h_ring = Ring(hg, hs_sem, hr_sem, y, ny, here, pending)
-    sub_rows = slots // r_subs
-    for sub in range(r_subs):
-        at = pl.ds(sub * sub_rows, sub_rows)
-        gate_pre = gacc[at]
-        up_pre = uacc[at]
-        for way, part in enumerate(r_ring.arrived(REACH)):
-            r_ring.serve_one(REACH, sub, way)
-            portion = rg[part, at]
-            gate_pre = gate_pre + dot(portion, gw[weight_rows(part), :])
-            up_pre = up_pre + dot(portion, uw[weight_rows(part), :])
-        hg[y, at] = (jax.nn.silu(gate_pre) * up_pre).astype(BF16)
-        h_ring.start(sub)
-
     dw_in.wait_recv()
-
-    def down(part, first):
-        total = dot(hg[part], dw[weight_rows(part), :])
-        if first:
-            oacc[...] = total
-        else:
-            oacc[...] += total
 
     def out_part(part, first):
         total = dot(ag[part, :rows], wog[part])
@@ -570,26 +581,24 @@
         else:
             macc[...] += total
 
-    down(y, True)
+    seven = [y]
+    for distance in range(1, half_ny):
+        seven += h_ring.arrived(distance)
+    for distance in range(3, half_ny):
+        for sub in ORDER:
+            h_ring.serve(distance, (sub,))
+            at = pl.ds(sub * sub_rows, sub_rows)
+            total = jnp.zeros((sub_rows, cols), F32)
+            for part in seven:
+                total = total + dot(hg[part, at], dw[weight_rows(part), :])
+            oacc[at] = total
+    a_ring.serve(1)
     wo_in.wait_recv()
     out_part(y, True)
-    for distance in range(1, half_ny):
-        h_ring.serve(distance)
-        if distance == 1:
-            a_ring.serve(1)
-        for part in h_ring.arrived(distance):
-            down(part, False)
-        if distance == 1:
-            for part in a_ring.arrived(1):
-                out_part(part, False)
-    a_ring.serve(2)
-
-    order = []
-    for sub in range(r_subs // 2):
-        order += [sub, sub + r_subs // 2]
+
     last = h_ring.arrived(half_ny)[0]
     back_own = pl.ds(pl.multiple_of(ep * cap, cap), cap)
-    for sub in order:
+    for sub in ORDER:
         for way in range(2):
             h_ring.serve_one(half_ny, sub, way)
         at = pl.ds(sub * sub_rows, sub_rows)
@@ -618,9 +627,9 @@
             send_partner(9, er.at[pl.ds(0, cap), other_lanes], ret.at[c, back_own])
     back_in = to_partner(9, er.at[pl.ds(0, cap), other_lanes], ret.at[other, back_own])
 
-    for part in a_ring.arrived(2):
+    for part in a_ring.arrived(1):
         out_part(part, False)
-    for distance in range(3, half_ny):
+    for distance in range(2, half_ny):
         a_ring.serve(distance)
         for part in a_ring.arrived(distance):
             out_part(part, False)
@@ -682,6 +691,10 @@
     for core in range(CORES):
         sent = ret.at[0, pl.ds(0, elsewhere)]
         pltpu.make_async_copy(sent, sent, back_send.at[core]).wait()
+    for ring in (x_ring, r_ring, h_ring, a_ring):
+        ring.finish()
+    pltpu.make_async_copy(wo_y_bytes, wo_y_bytes, wo_send.at[0]).wait()
+    pltpu.make_async_copy(wo_x_bytes, wo_x_bytes, wo_send.at[1]).wait()
     for copy in pending:
         copy.wait_send()
 
@@ -725,12 +738,11 @@
     units = expert_gate.shape[2] * CORES
     a_rows = rows + toks // CORES
     dma = pltpu.SemaphoreType.DMA
-    vmem = pl.BlockSpec(memory_space=pltpu.VMEM)
-    smem = pl.BlockSpec(memory_space=pltpu.SMEM)
-    hbm = pl.BlockSpec(memory_space=pl.ANY)
-
-    def ring_sems(subs):
-        return [dma((2, ny // 2, subs)), dma((2, ny // 2, subs))]
+    hbm = pl.BlockSpec(memory_space=pltpu.HBM)
+    anywhere = pl.BlockSpec(memory_space=pl.ANY)
+
+    def ring_sems(subs, parts):
+        return [dma(()), dma((subs * parts,))]
 
     return pl.pallas_call(
         functools.partial(kernel, n_ep, ny, nx),
@@ -739,30 +751,17 @@
             jax.ShapeDtypeStruct((rows_all, mine), BF16),
             jax.ShapeDtypeStruct((toks, mine), BF16),
         ),
-        in_specs=[
-            hbm,
-            vmem,
-            hbm,
-            hbm,
-            hbm,
-            vmem,
-            vmem,
-            smem,
-            hbm,
-            hbm,
-            vmem,
-            vmem,
-            vmem,
-            hbm,
-            hbm,
-            hbm,
-            hbm,
-            hbm,
-            hbm,
-        ],
-        out_specs=(hbm, hbm),
+        in_specs=[hbm] * 19,
+        out_specs=(anywhere, anywhere),
         scratch_shapes=[
             pltpu.VMEM((ny, rows, cols), BF16),
+            pltpu.VMEM((1, dim), F32),
+            pltpu.VMEM((1, HEAD), F32),
+            pltpu.VMEM((1, HEAD), F32),
+            pltpu.SMEM((1,), F32),
+            pltpu.VMEM((1, dim), F32),
+            pltpu.VMEM(route_ids.shape[::-1], jnp.int32),
+            pltpu.VMEM(route_ids.shape[::-1], F32),
             pltpu.VMEM((rows, mine), BF16),
             pltpu.VMEM((toks, dim), BF16),
             pltpu.VMEM(w_key.shape, BF16),
@@ -786,8 +785,6 @@
             pltpu.VMEM((rows, cols), F32),
             pltpu.VMEM((toks, mine), BF16),
             pltpu.VMEM((toks, dim), BF16),
-            pltpu.VMEM((slots, units), F32),
-            pltpu.VMEM((slots, units), F32),
             pltpu.VMEM((slots, cols), F32),
             pltpu.VMEM((rows, 2 * HEAD), F32),
             pltpu.VMEM((rows, 2 * HEAD), F32),
@@ -798,21 +795,21 @@
             pltpu.VMEM((3, rows, mine), BF16),
             pltpu.VMEM((ny, toks // CORES, 2 * HEAD), BF16),
         ]
-        + ring_sems(4)
-        + ring_sems(4)
-        + ring_sems(4)
-        + ring_sems(2)
+        + ring_sems(SUBS, ny - 1)
+        + ring_sems(SUBS, 2 * REACH)
+        + ring_sems(SUBS, ny - 1)
+        + ring_sems(2, ny - 1)
         + [
-            dma((13,)),
+            dma((20,)),
             dma((12,)),
             dma((12,)),
             dma((ny - 2 * REACH,)),
-            dma((4 + ny - 1 - 2 * REACH,)),
+            dma((2 * SUBS,)),
             dma((2,)),
             dma((2,)),
             dma(()),
-            dma((ny - 1 + nx - 1,)),
-            dma((ny - 1 + nx - 1,)),
+            dma((2,)),
+            dma((2,)),
             dma(()),
             dma(()),
             dma((3,)),

time: 84.2 us -> 80 us (0.950)
  Pallas kernels: 80.5 us -> 76.4 us
    pallas_call x1, Pallas kernels: 80.5 us -> 76.4 us  [shards(): pl.pallas_call(functools.partial(kernel, n_ep, ny, nx), name='layer', out...]
where the time goes in v3:
time: 80 us; the launch traced here: 79.8 us
  Pallas kernels  76.4 us (96%)
  local copies, waits for them, and re-layouts  2.19 us (3%)
  between operations  1.3 us (2%)
    pallas_call x1, Pallas kernels, shards(): pl.pallas_call(functools.partial(kernel, n_ep, ny, nx), name='layer', out...  76.4 us
    unnamed x4, local copies, waits for them, and re-layouts  2.19 us

profile of v3, /device:TPU:1, one launch (start us, length us, event | category | flops | bytes accessed | tf_op | source)
XLA Modules:
  0.0 79.8 jit_solution(16006241099233681249)
XLA Ops:
  1.3 76.4 %layer.1 = (bf16[512,128]{1,0:T(8,128)(2,1)}, bf16[128,128]{1,0:T(8,128)(2,1)}) custom-call(bf16[512,128]{1,0:T(8,128)(2,1)} %x_ref.1, f32[1,2048]{1,0:T(1,128)} %bitcast.12, bf16[64,2048]{1,0:T(8,128)(2,1)} %bitcast.9, bf16[2048,128]{1,0:T(8,128)(2,1)} %wk_ref.1, bf16[2048,128]{1,0:T(8,128)(2,1)} %wv_ref.1, f32[1,64]{1,0:T(1,128)} %bitcast.16, ...), custom_call_target="tpu_custom_call" | custom-call | tf_op jit(solution)/shard_map/layer/pallas_call | solution.py:747
  77.6 0.0 copy-start
  77.7 1.6 %copy.24 = bf16[512,128]{1,0:T(8,128)(2,1)} copy(bf16[512,128]{1,0:T(8,128)(2,1)} %get-tuple-element.4) | data formatting | bytes 262144
  79.2 0.0 copy-done
  79.2 0.6 copy.25
Async XLA Ops:
  77.6 1.6 %copy-start = (bf16[128,128]{1,0:T(8,128)(2,1)S(1)}, bf16[128,128]{1,0:T(8,128)(2,1)}, u32[]{:S(2)}) copy-start(bf16[128,128]{1,0:T(8,128)(2,1)} %get-tuple-element.5) | copy-start | bytes 98308

commit v4 on v3

--- a/solution.py
+++ b/solution.py
@@ -15,6 +15,7 @@
 REACH = 2
 SUBS = 4
 ORDER = (0, 3, 1, 2)
+FURTHER = ()
 F32 = jnp.float32
 BF16 = jnp.bfloat16
 MESH = pl.DeviceIdType.MESH
@@ -33,7 +34,8 @@
 
 
 class Ring:
-    def __init__(self, buf, send_sem, recv_sem, y, ny, place, subs, reach=None):
+    def __init__(self, buf, send_sem, recv_sem, y, ny, place, subs, reach=None, further=()):
+        self.further = further
         self.buf, self.send_sem, self.recv_sem = buf, send_sem, recv_sem
         self.y, self.ny, self.place = y, ny, place
         self.subs, self.reach = subs, reach
@@ -42,7 +44,7 @@
 
     def carries(self, way, distance, sub):
         if self.reach is not None:
-            return distance <= self.reach
+            return distance <= self.reach + (sub in self.further)
         if distance < self.half:
             return True
         if distance > self.half:
@@ -89,8 +91,11 @@
         return [mod(self.y - distance, self.ny)]
 
     def finish(self):
-        count = self.ny - 1 if self.reach is None else 2 * self.reach
-        sent = self.buf.at[pl.ds(0, count)]
+        pieces = (self.ny - 1) * self.subs
+        if self.reach is not None:
+            pieces = 2 * (self.reach * self.subs + len(self.further))
+        high = max(k for k in range(1, self.subs + 1) if pieces % k == 0)
+        sent = self.buf.at[pl.ds(0, pieces // high), pl.ds(0, high * self.rows)]
         pltpu.make_async_copy(sent, sent, self.send_sem).wait()
 
 
@@ -242,7 +247,8 @@
             )
         return carry
 
-    lax.fori_loop(1, n_ep, greet, 0)
+    lax.fori_loop(n_ep // 4, n_ep, greet, 0)
+    lax.fori_loop(1, n_ep // 4, greet, 0)
     for k in range(1, ny):
         pl.semaphore_signal(barrier, inc=1, device_id=here(mod(y + k, ny)), device_id_type=MESH)
     pl.semaphore_signal(barrier, inc=1, device_id=partner, device_id_type=MESH)
@@ -312,28 +318,37 @@
     send_partner(0, xv, xg.at[y, :, own_lanes])
     x_in = to_partner(0, xv, xg.at[y, :, other_lanes])
 
+    zi = ep // nx
+    nz = n_ep // nx
+    away = zi > 0
     wov_in.wait()
+    wo_place = mod(y + zi, ny)
     wo_self = pltpu.make_async_copy(
-        wov.at[wo_src, lanes_of(y)], wog.at[y, wo_dst], local_sem.at[3]
+        wov.at[wo_src, lanes_of(wo_place)], wog.at[y, wo_dst], local_sem.at[3]
     )
-    wo_self.start()
-
-    def wo_y(k, part):
-        place = mod(y + k, ny)
-        return pltpu.make_async_remote_copy(
-            src_ref=wov.at[wo_src, lanes_of(place)],
-            dst_ref=wog.at[part, wo_dst],
-            send_sem=wo_send.at[0],
-            recv_sem=wo_recv.at[0],
-            device_id=here(place),
-            device_id_type=MESH,
-        )
-
-    for k in range(1, ny):
-        wo_y(k, y).start()
+    wo_y = pltpu.make_async_remote_copy(
+        src_ref=wov.at[wo_src, lanes_of(wo_place)],
+        dst_ref=wog.at[y, wo_dst],
+        send_sem=wo_send.at[0],
+        recv_sem=wo_recv.at[0],
+        device_id=here(wo_place),
+        device_id_type=MESH,
+    )
+
+    @pl.when(away)
+    def _():
+        wo_y.start()
+
+    @pl.when(jnp.logical_not(away))
+    def _():
+        wo_self.start()
+
     r_subs = SUBS
     sub_rows = slots // r_subs
     per_sub = n_ep // r_subs
+
+    def direct(far, sub):
+        return sub not in FURTHER or 0 < far < len(far_parts) - 1
 
     def dispatch(blocks, parts, base):
         for block, part in zip(blocks, parts):
@@ -348,6 +363,8 @@
             def send(k, carry, sub=sub):
                 target = lax.rem(ep + n_ep - k, n_ep)
                 for block, part in zip(blocks, parts):
+                    if base and not direct(block - 1, sub):
+                        continue
                     pltpu.make_async_remote_copy(
                         src_ref=og.at[block, pl.ds(pl.multiple_of(target * cap, cap), cap)],
                         dst_ref=rg.at[part, pl.ds(pl.multiple_of(k * cap, cap), cap)],
@@ -369,6 +386,7 @@
 
     for k, part in enumerate(far_parts):
         og[k + 1] = dot(pick, normed[:, lanes_of(part)]).astype(BF16)
+    dispatch(range(1, len(far_parts) + 1), far_parts, r_subs)
 
     for copy in weights_in + small:
         copy.wait()
@@ -379,13 +397,12 @@
 
     x_ring.serve(1)
 
-    dispatch(range(1, len(far_parts) + 1), far_parts, r_subs)
     send_partner(1, gw.at[:, own_lanes], gw.at[:, own_lanes])
     send_partner(2, uw.at[:, own_lanes], uw.at[:, own_lanes])
     gw_in = to_partner(1, gw.at[:, own_lanes], gw.at[:, other_lanes])
     uw_in = to_partner(2, uw.at[:, own_lanes], uw.at[:, other_lanes])
 
-    r_ring = Ring(rg, rs_sem, rr_sem, y, ny, here, r_subs, REACH)
+    r_ring = Ring(rg, rs_sem, rr_sem, y, ny, here, r_subs, REACH, FURTHER)
 
     def r_start(sub):
         landed = rg.at[y, pl.ds(sub * per_sub * cap, per_sub * cap)]
@@ -398,26 +415,6 @@
 
     for sub in ORDER[1:]:
         r_start(sub)
-
-    wo_y_bytes = og.at[0, pl.ds(0, (ny - 1) * wo_piece)]
-    pltpu.make_async_copy(wo_y_bytes, wo_y_bytes, wo_recv.at[0]).wait()
-    wo_self.wait()
-
-    def wo_x(k, sender):
-        place = ep - xi + lax.rem(xi + k, nx)
-        piece = pl.ds(pl.multiple_of(c * wo_rows + sender * wo_piece, wo_piece), wo_piece)
-        return pltpu.make_async_remote_copy(
-            src_ref=wog.at[:, piece],
-            dst_ref=wog.at[:, piece],
-            send_sem=wo_send.at[1],
-            recv_sem=wo_recv.at[1],
-            device_id=(place, tp),
-            device_id_type=MESH,
-        )
-
-    wo_x_bytes = wog.at[:, pl.ds(0, (nx - 1) * wo_piece)]
-    for k in range(1, nx):
-        wo_x(k, xi).start()
 
     x_ring.serve(3)
     send_partner(4, sgs.at[own_head], sgs.at[own_head])
@@ -439,8 +436,12 @@
 
     def hidden(sub):
         for way in range(2):
-            r_ring.serve_one(REACH, sub, way)
-        landed = rg.at[pl.ds(0, len(far_parts)), pl.ds(0, sub_rows)]
+            if sub in FURTHER:
+                r_ring.serve_one(REACH + 1, sub, way)
+            else:
+                r_ring.serve_one(REACH, sub, way)
+        n_direct = sum(direct(far, sub) for far in range(len(far_parts)))
+        landed = rg.at[pl.ds(0, n_direct), pl.ds(0, sub_rows)]
         pltpu.make_async_copy(landed, landed, disp_recv.at[r_subs + sub]).wait()
         at = pl.ds(sub * sub_rows, sub_rows)
         gate_pre = jnp.zeros((sub_rows, gw.shape[1]), F32)
@@ -513,6 +514,10 @@
     @pl.when(leads)
     def _():
         kv[:, :WINDOW] = jnp.zeros((2, WINDOW, HEAD), BF16)
+
+    for sub in FURTHER:
+        for way in range(2):
+            r_ring.serve_one(REACH, sub, way)
 
     hidden(ORDER[2])
     h_ring.serve(1, ORDER[:2])
@@ -556,8 +561,34 @@
             heads.append(dot(probs, kv[1, start : start + 2 * WINDOW]))
         ag[y, start : start + WINDOW] = jnp.concatenate(heads, axis=1).astype(BF16)
 
+    wo_part = mod(y - zi, ny)
+
+    @pl.when(away)
+    def _():
+        wo_y.wait()
+
+    @pl.when(jnp.logical_not(away))
+    def _():
+        wo_self.wait()
+
+    wo_z_bytes = og.at[0, pl.ds(0, (nz - 1) * wo_piece)]
+    for k in range(1, nz):
+        pltpu.make_async_remote_copy(
+            src_ref=wog.at[wo_part, wo_dst],
+            dst_ref=wog.at[wo_part, wo_dst],
+            send_sem=wo_send.at[1],
+            recv_sem=wo_recv.at[1],
+            device_id=(lax.rem(ep + k * nx, n_ep), tp),
+            device_id_type=MESH,
+        ).start()
+
     for block in range(rows // WINDOW):
         attend(block)
+
+    a_ring = Ring(ag, as_sem, ar_sem, y, ny, here, 2)
+    for sub in range(a_ring.subs):
+        a_ring.start(sub)
+
     hidden(ORDER[3])
 
     h_ring.serve(1, ORDER[2:3])
@@ -565,14 +596,17 @@
     h_ring.serve(1, ORDER[3:])
     h_ring.serve(2, ORDER[2:])
 
-    a_ring = Ring(ag, as_sem, ar_sem, y, ny, here, 2)
-    for sub in range(a_ring.subs):
-        a_ring.start(sub)
-
-    pltpu.make_async_copy(wo_x_bytes, wo_x_bytes, wo_recv.at[1]).wait()
-    send_partner(8, wog.at[:, wo_own], wog.at[:, wo_own])
-    wo_in = to_partner(8, wog.at[:, wo_other], wog.at[:, wo_other])
-    dw_in.wait_recv()
+    pltpu.make_async_copy(wo_z_bytes, wo_z_bytes, wo_recv.at[1]).wait()
+    wo_x_bytes = wog.at[:, pl.ds(0, (nx - 1) * wo_piece)]
+    for k in range(1, nx):
+        pltpu.make_async_remote_copy(
+            src_ref=wog.at[:, wo_dst],
+            dst_ref=wog.at[:, wo_dst],
+            send_sem=wo_send.at[2],
+            recv_sem=wo_recv.at[2],
+            device_id=(ep - xi + lax.rem(xi + k, nx), tp),
+            device_id_type=MESH,
+        ).start()
 
     def out_part(part, first):
         total = dot(ag[part, :rows], wog[part])
@@ -580,6 +614,9 @@
             macc[...] = total
         else:
             macc[...] += total
+
+    a_ring.serve(1)
+    dw_in.wait_recv()
 
     seven = [y]
     for distance in range(1, half_ny):
@@ -592,9 +629,12 @@
             for part in seven:
                 total = total + dot(hg[part, at], dw[weight_rows(part), :])
             oacc[at] = total
-    a_ring.serve(1)
-    wo_in.wait_recv()
-    out_part(y, True)
+    a_ring.serve(2)
+
+    pltpu.make_async_copy(wo_x_bytes, wo_x_bytes, wo_recv.at[2]).wait()
+    send_partner(8, wog.at[:, wo_own], wog.at[:, wo_own])
+    wo_in = to_partner(8, wog.at[:, wo_other], wog.at[:, wo_other])
+
 
     last = h_ring.arrived(half_ny)[0]
     back_own = pl.ds(pl.multiple_of(ep * cap, cap), cap)
@@ -627,9 +667,12 @@
             send_partner(9, er.at[pl.ds(0, cap), other_lanes], ret.at[c, back_own])
     back_in = to_partner(9, er.at[pl.ds(0, cap), other_lanes], ret.at[other, back_own])
 
-    for part in a_ring.arrived(1):
-        out_part(part, False)
-    for distance in range(2, half_ny):
+    wo_in.wait_recv()
+    out_part(y, True)
+    for distance in range(1, 3):
+        for part in a_ring.arrived(distance):
+            out_part(part, False)
+    for distance in range(3, half_ny):
         a_ring.serve(distance)
         for part in a_ring.arrived(distance):
             out_part(part, False)
@@ -686,15 +729,18 @@
     mo_second.start()
 
     for block in range(len(far_parts) + 1):
-        sent = og.at[block, pl.ds(0, elsewhere)]
+        count = elsewhere
+        if block:
+            count -= sub_rows * sum(not direct(block - 1, sub) for sub in range(r_subs))
+        sent = og.at[block, pl.ds(0, count)]
         pltpu.make_async_copy(sent, sent, disp_send.at[block]).wait()
     for core in range(CORES):
         sent = ret.at[0, pl.ds(0, elsewhere)]
         pltpu.make_async_copy(sent, sent, back_send.at[core]).wait()
     for ring in (x_ring, r_ring, h_ring, a_ring):
         ring.finish()
-    pltpu.make_async_copy(wo_y_bytes, wo_y_bytes, wo_send.at[0]).wait()
-    pltpu.make_async_copy(wo_x_bytes, wo_x_bytes, wo_send.at[1]).wait()
+    pltpu.make_async_copy(wo_z_bytes, wo_z_bytes, wo_send.at[1]).wait()
+    pltpu.make_async_copy(wo_x_bytes, wo_x_bytes, wo_send.at[2]).wait()
     for copy in pending:
         copy.wait_send()
 
@@ -808,8 +854,8 @@
             dma((2,)),
             dma((2,)),
             dma(()),
-            dma((2,)),
-            dma((2,)),
+            dma((3,)),
+            dma((3,)),
             dma(()),
             dma(()),
             dma((3,)),

time: 80 us -> 78.7 us (0.984)
  Pallas kernels: 76.4 us -> 75 us
    pallas_call x1, Pallas kernels: 76.4 us -> 75 us  [shards(): pl.pallas_call(functools.partial(kernel, n_ep, ny, nx), name='layer', out...]
where the time goes in v4:
time: 78.7 us; the launch traced here: 78.5 us
  Pallas kernels  75 us (95%)
  local copies, waits for them, and re-layouts  2.19 us (3%)
  between operations  1.3 us (2%)
    pallas_call x1, Pallas kernels, shards(): pl.pallas_call(functools.partial(kernel, n_ep, ny, nx), name='layer', out...  75 us
    unnamed x4, local copies, waits for them, and re-layouts  2.19 us

profile of v4, /device:TPU:1, one launch (start us, length us, event | category | flops | bytes accessed | tf_op | source)
XLA Modules:
  0.0 78.5 jit_solution(7663316355697470600)
XLA Ops:
  1.3 75.0 %layer.1 = (bf16[512,128]{1,0:T(8,128)(2,1)}, bf16[128,128]{1,0:T(8,128)(2,1)}) custom-call(bf16[512,128]{1,0:T(8,128)(2,1)} %x_ref.1, f32[1,2048]{1,0:T(1,128)} %bitcast.12, bf16[64,2048]{1,0:T(8,128)(2,1)} %bitcast.9, bf16[2048,128]{1,0:T(8,128)(2,1)} %wk_ref.1, bf16[2048,128]{1,0:T(8,128)(2,1)} %wv_ref.1, f32[1,64]{1,0:T(1,128)} %bitcast.16, ...), custom_call_target="tpu_custom_call" | custom-call | tf_op jit(solution)/shard_map/layer/pallas_call | solution.py:793
  76.3 0.0 copy-start
  76.3 1.6 %copy.24 = bf16[512,128]{1,0:T(8,128)(2,1)} copy(bf16[512,128]{1,0:T(8,128)(2,1)} %get-tuple-element.4) | data formatting | bytes 262144
  77.9 0.0 copy-done
  77.9 0.6 copy.25
Async XLA Ops:
  76.3 1.6 %copy-start = (bf16[128,128]{1,0:T(8,128)(2,1)S(1)}, bf16[128,128]{1,0:T(8,128)(2,1)}, u32[]{:S(2)}) copy-start(bf16[128,128]{1,0:T(8,128)(2,1)} %get-tuple-element.5) | copy-start | bytes 98308

commit v5 on v4

--- a/solution.py
+++ b/solution.py
@@ -16,6 +16,7 @@
 SUBS = 4
 ORDER = (0, 3, 1, 2)
 FURTHER = ()
+PAIR_SEM = {1: 0, 2: 0, 7: 0, 3: 1, 4: 1, 5: 1, 8: 1, 0: 2, 10: 2, 11: 2, 6: 3, 9: 3}
 F32 = jnp.float32
 BF16 = jnp.bfloat16
 MESH = pl.DeviceIdType.MESH
@@ -200,7 +201,6 @@
     cap = er.shape[0] // n_ep
     slots = er.shape[0]
     xi = lax.rem(ep, nx)
-    pending = []
     far_parts = [mod(y + REACH + 1 + k, ny) for k in range(ny - 1 - 2 * REACH)]
 
     def here(place):
@@ -304,16 +304,14 @@
         return pltpu.make_async_remote_copy(
             src_ref=source,
             dst_ref=target,
-            send_sem=pair_send.at[index],
+            send_sem=pair_send.at[PAIR_SEM[index]],
             recv_sem=pair_recv.at[index],
             device_id=partner,
             device_id_type=MESH,
         )
 
     def send_partner(index, source, target):
-        copy = to_partner(index, source, target)
-        copy.start()
-        pending.append(copy)
+        to_partner(index, source, target).start()
 
     send_partner(0, xv, xg.at[y, :, own_lanes])
     x_in = to_partner(0, xv, xg.at[y, :, other_lanes])
@@ -741,8 +739,9 @@
         ring.finish()
     pltpu.make_async_copy(wo_z_bytes, wo_z_bytes, wo_send.at[1]).wait()
     pltpu.make_async_copy(wo_x_bytes, wo_x_bytes, wo_send.at[2]).wait()
-    for copy in pending:
-        copy.wait_send()
+    pair_sent = [hg.at[pl.ds(0, 6)], hg.at[pl.ds(0, 4)], hg.at[0], og.at[0, pl.ds(0, 16)]]
+    for index, sent in enumerate(pair_sent):
+        pltpu.make_async_copy(sent, sent, pair_send.at[index]).wait()
 
     @pl.when(jnp.logical_not(trails))
     def _():
@@ -847,7 +846,7 @@
         + ring_sems(2, ny - 1)
         + [
             dma((20,)),
-            dma((12,)),
+            dma((4,)),
             dma((12,)),
             dma((ny - 2 * REACH,)),
             dma((2 * SUBS,)),

time: 78.7 us -> 78.6 us (level)
  no operation moved by 1% of the time
where the time goes in v5:
time: 78.6 us; the launch traced here: 78.5 us
  Pallas kernels  75 us (95%)
  local copies, waits for them, and re-layouts  2.19 us (3%)
  between operations  1.3 us (2%)
    pallas_call x1, Pallas kernels, shards(): pl.pallas_call(functools.partial(kernel, n_ep, ny, nx), name='layer', out...  75 us
    unnamed x4, local copies, waits for them, and re-layouts  2.19 us

profile of v5, /device:TPU:1, one launch (start us, length us, event | category | flops | bytes accessed | tf_op | source)
XLA Modules:
  0.0 78.5 jit_solution(9757992090156074838)
XLA Ops:
  1.3 75.0 %layer.1 = (bf16[512,128]{1,0:T(8,128)(2,1)}, bf16[128,128]{1,0:T(8,128)(2,1)}) custom-call(bf16[512,128]{1,0:T(8,128)(2,1)} %x_ref.1, f32[1,2048]{1,0:T(1,128)} %bitcast.12, bf16[64,2048]{1,0:T(8,128)(2,1)} %bitcast.9, bf16[2048,128]{1,0:T(8,128)(2,1)} %wk_ref.1, bf16[2048,128]{1,0:T(8,128)(2,1)} %wv_ref.1, f32[1,64]{1,0:T(1,128)} %bitcast.16, ...), custom_call_target="tpu_custom_call" | custom-call | tf_op jit(solution)/shard_map/layer/pallas_call | solution.py:792
  76.3 0.0 copy-start
  76.3 1.6 %copy.24 = bf16[512,128]{1,0:T(8,128)(2,1)} copy(bf16[512,128]{1,0:T(8,128)(2,1)} %get-tuple-element.4) | data formatting | bytes 262144
  77.8 0.0 copy-done
  77.8 0.6 copy.25
Async XLA Ops:
  76.3 1.6 %copy-start = (bf16[128,128]{1,0:T(8,128)(2,1)S(1)}, bf16[128,128]{1,0:T(8,128)(2,1)}, u32[]{:S(2)}) copy-start(bf16[128,128]{1,0:T(8,128)(2,1)} %get-tuple-element.5) | copy-start | bytes 98308
